TPU v7x, 32 devices: a whole 2x2x4 slice. The times are simulated.
32 devices in a mesh: sp: 8 (over z, y), tp: 4 (over x, core).
Axes of the slice: x: 2, y: 2, z: 4, core: 2. Of those that a mesh axis runs over, the one named last changes fastest.
Arguments:
- residual: bfloat16 [8192, 2048], P(('sp', 'tp')), may hold values from -6 to 6
- first_group_queries: bfloat16 [8192, 1024], P('sp', 'tp'), may hold values from -6 to 6
- first_group_keys: bfloat16 [8192, 1024], P('sp', 'tp'), may hold values from -6 to 6
- second_group_queries: bfloat16 [8192, 512], P('sp', 'tp'), may hold values from -6 to 6
- second_group_keys: bfloat16 [8192, 512], P('sp', 'tp'), may hold values from -6 to 6
- primary_retain_switch_inputs: bfloat16 [8192, 1024], P('sp', 'tp'), may hold values from -12 to 16
- secondary_retain_switch_inputs: bfloat16 [8192, 512], P('sp', 'tp'), may hold values from -12 to 16
- timestep_fading_exponent: float32 [8192], P('sp'), may hold values from -2.1 to 0
- values: bfloat16 [2, 8192, 1024], P(None, 'sp', 'tp'), may hold values from -6 to 6
- output_gate_logits: bfloat16 [2, 8192, 1024], P(None, 'sp', 'tp'), may hold values from -6 to 6
- head_norm_gains: float32 [2, 1024], P(None, 'tp'), may hold values from 0.1 to 1.9
- output_projection: bfloat16 [2, 1024, 2048], P(None, 'tp'), may hold values from -0.125 to 0.125
- feedforward_norm_gain: float32 [2048], replicated, may hold values from 0.1 to 1.9
- gate_projection: bfloat16 [2048, 6144], P('sp', 'tp'), may hold values from -0.125 to 0.125
- up_projection: bfloat16 [2048, 6144], P('sp', 'tp'), may hold values from -0.125 to 0.125
- down_projection: bfloat16 [6144, 2048], P('tp', 'sp'), may hold values from -0.078125 to 0.078125
Outputs:
- layer_out: bfloat16 [8192, 2048], P(('sp', 'tp'))
All inputs are finite; a program needn't handle non-finite values.
Results may differ from a plain program's by a relative error of at most 0.018.
Values may be sent and summed in bfloat16 or wider, within the bound.
A program may use at most 128 MiB of HBM per device.

v0:
```python
import functools

import jax
import jax.numpy as jnp
from jax import lax
from jax.experimental import pallas as pl
from jax.experimental.pallas import tpu as pltpu
from jax.sharding import PartitionSpec as P

FIRST_KEY_SIZE = 128
SECOND_KEY_SIZE = 64
DV = 128
CHUNK = 128
MIDDLE = CHUNK // 2 - 1
PAD = 16
MESH = pl.DeviceIdType.MESH

EPS = 1e-06
SOFTNESS_SCALE = 16.0
VMEM_BYTES = 66_000_000

def dot(a, b, dims):
    return lax.dot_general(a, b, (dims, ((), ())), preferred_element_type=jnp.float32)


def positions():
    row = lax.broadcasted_iota(jnp.int32, (CHUNK, CHUNK), 0)
    column = lax.broadcasted_iota(jnp.int32, (CHUNK, CHUNK), 1)
    return row, column


def fading_sums(fading_row):
    row, column = positions()
    as_column = jnp.sum(jnp.where(row == column, fading_row, 0.0), axis=1, keepdims=True)
    column_sums = jnp.sum(jnp.where(column <= row, fading_row, 0.0), axis=1, keepdims=True)
    row_sums = jnp.sum(jnp.where(row <= column, as_column, 0.0), axis=0, keepdims=True)
    return column_sums, row_sums


def channel_sums(switches):
    row, column = positions()
    x = switches.astype(jnp.float32)
    logs = (jnp.minimum(x, 0.0) - jnp.log1p(jnp.exp(-jnp.abs(x)))) * (1.0 / SOFTNESS_SCALE)
    lower = (column <= row).astype(jnp.bfloat16)
    high = logs.astype(jnp.bfloat16)
    low = (logs - high.astype(jnp.float32)).astype(jnp.bfloat16)
    return dot(lower, high, ((1,), (0,))) + dot(lower, low, ((1,), (0,)))


def lanes_of(head, width, key_width):
    lane = lax.broadcasted_iota(jnp.int32, (1, width), 1)
    return (lane >= head * key_width) & (lane < (head + 1) * key_width)


def advanced(state, inverse_keys, weighted, sums, total_fading, key_width):
    width = state.shape[1]
    end, middle = sums[CHUNK - 1 :, :], sums[MIDDLE : MIDDLE + 1, :]
    head_count = width // key_width
    if key_width % 128 == 0:
        added = jnp.concatenate(
            [
                dot(
                    weighted[:, h * DV : (h + 1) * DV],
                    inverse_keys[:, h * key_width : (h + 1) * key_width],
                    ((0,), (0,)),
                )
                for h in range(head_count)
            ],
            axis=1,
        )
    else:
        added = jnp.zeros((DV, width), jnp.float32)
        for h in range(head_count):
            product = dot(weighted[:, h * DV : (h + 1) * DV], inverse_keys, ((0,), (0,)))
            added = jnp.where(lanes_of(h, width, key_width), product, added)
    return jnp.exp(end + total_fading) * state + jnp.exp(end - middle) * added


def remote(source, target, send, receive, device):
    return pltpu.make_async_remote_copy(
        src_ref=source,
        dst_ref=target,
        send_sem=send,
        recv_sem=receive,
        device_id=device,
        device_id_type=MESH,
    )


def rows_at(index, count):
    return pl.ds(pl.multiple_of(index * count, count), count)


class Ring:
    def __init__(self, peers, place, tp_place, gate, up, down, gate_sems, down_sems):
        self.peers, self.tp_place = peers, tp_place
        self.gate, self.up, self.down = gate, up, down
        self.gate_sems, self.down_sems = gate_sems, down_sems
        self.position = jnp.where(place % 2 == 0, place // 2, peers - 1 - place // 2)
        self.full = (peers - 1) // 2
        self.hops = peers // 2
        self.beyond = (self.origin(0, -1), self.origin(1, -1))
        self.waited = set()
        self.issued = 0
        self.events = ([], [])
        for way in (0, 1):
            for matrix, count in ((0, 4), (1, 2)):
                for hop in range(1, self.hops + 1):
                    for piece in self.carried(way, hop, count):
                        self.events[way].append((matrix, hop, piece))

    def origin(self, way, distance):
        place = (self.position + (distance if way else -distance) + 2 * self.peers) % self.peers
        return jnp.where(place < (self.peers + 1) // 2, 2 * place, 2 * (self.peers - 1 - place) + 1)

    def carried(self, way, hop, count):
        if hop <= self.full:
            return range(count)
        return range(count // 2, count) if way else range(count // 2)

    def piece(self, matrix, origin, piece):
        if matrix:
            half = self.down.shape[1] // 2
            return self.down.at[origin, pl.ds(piece * half, half), :]
        half = self.gate.shape[0] // self.peers // 2
        return (self.up if piece // 2 else self.gate).at[rows_at(origin * 2 + piece % 2, half), :]

    def copy(self, way, matrix, hop, piece, distance):
        ref = self.piece(matrix, self.origin(way, distance), piece)
        send, receive = self.down_sems if matrix else self.gate_sems
        at = (way, hop - 1, piece)
        return remote(ref, ref, send.at[at], receive.at[at], (self.beyond[way], self.tp_place))

    def arrive(self, way, matrix, hop, piece):
        if (way, matrix, hop, piece) not in self.waited:
            self.waited.add((way, matrix, hop, piece))
            self.copy(way, matrix, hop, piece, hop).wait_recv()

    def pump(self, until):
        until = len(self.events[0]) if until is None else (until * len(self.events[0]) + 20) // 21
        while self.issued < until:
            for way in (0, 1):
                matrix, hop, piece = self.events[way][self.issued]
                if hop > 1:
                    self.arrive(way, matrix, hop - 1, piece)
                self.copy(way, matrix, hop, piece, hop - 1).start()
            self.issued += 1

    def arrive_gates(self):
        for hop in range(1, self.hops + 1):
            for way in (0, 1):
                for piece in self.carried(way, hop, 4):
                    self.arrive(way, 0, hop, piece)

    def finish(self):
        for way in (0, 1):
            for matrix, hop, piece in self.events[way]:
                self.copy(way, matrix, hop, piece, hop - 1).wait_send()


def layer_kernel(
    n_sp,
    n_tp,
    residual_hbm,
    qa_hbm,
    qb_hbm,
    ka_hbm,
    kb_hbm,
    sa_hbm,
    sb_hbm,
    values_hbm,
    gates_hbm,
    projection_hbm,
    gate_hbm,
    up_hbm,
    down_hbm,
    fading,
    gains,
    row_gain,
    mid,
    down_sum,
    residual,
    qa,
    qb,
    ka,
    kb,
    sa,
    sb,
    values,
    gates,
    projection,
    gate_full,
    up_full,
    down_full,
    sums_a,
    sums_b,
    before_a,
    before_b,
    starts,
    heads,
    state_a,
    state_b,
    decay,
    packs,
    pair_got,
    later_got,
    terms,
    partner_terms,
    cross_terms,
    cross_got,
    own_sum,
    all_rows,
    hidden,
    stage,
    stage_partner,
    stage_cross,
    stage_got,
    load_sems,
    gate_send,
    gate_receive,
    down_send,
    down_receive,
    pair_sems,
    later_send,
    later_receive,
    terms_send,
    terms_receive,
    cross_send,
    cross_receive,
    rows_send,
    rows_receive,
    passed_send,
    passed_receive,
    half_send,
    half_receive,
    last_send,
    last_receive,
):
    place, tp_place = lax.axis_index("sp"), lax.axis_index("tp")
    chip, core = tp_place // 2, tp_place % 2
    chips = n_tp // 2
    partner = (place, 2 * chip + 1 - core)
    rows, own_rows = qa.shape[0], residual.shape[0]
    chunks, units = rows // CHUNK, own_rows // CHUNK
    width_a, width_b = ka.shape[1], kb.shape[1]
    width = width_a + width_b
    groups = (
        (qa, ka, sa, sums_a, before_a, state_a, FIRST_KEY_SIZE, 0),
        (qb, kb, sb, sums_b, before_b, state_b, SECOND_KEY_SIZE, width_a),
    )
    inner = gate_hbm.shape[0]

    barrier = pltpu.get_barrier_semaphore()
    for k in range(1, n_sp):
        pl.semaphore_signal(
            barrier, inc=1, device_id=((place + k) % n_sp, tp_place), device_id_type=MESH
        )
    for k in range(1, n_tp):
        pl.semaphore_signal(
            barrier, inc=1, device_id=(place, (tp_place + k) % n_tp), device_id_type=MESH
        )

    loads = [
        (gate_hbm, gate_full.at[rows_at(place, inner), :]),
        (up_hbm, up_full.at[rows_at(place, inner), :]),
        (ka_hbm, ka),
        (kb_hbm, kb),
        (sa_hbm, sa),
        (sb_hbm, sb),
        (values_hbm, values),
        (qa_hbm, qa),
        (qb_hbm, qb),
        (down_hbm, down_full.at[place]),
        (projection_hbm, projection),
        (gates_hbm, gates),
        (residual_hbm, residual),
    ]
    loads = [pltpu.make_async_copy(a, b, load_sems.at[i]) for i, (a, b) in enumerate(loads)]
    for load in loads:
        load.start()
    ring = Ring(
        n_sp,
        place,
        tp_place,
        gate_full,
        up_full,
        down_full,
        (gate_send, gate_receive),
        (down_send, down_receive),
    )
    state_a[...] = jnp.zeros_like(state_a)
    state_b[...] = jnp.zeros_like(state_b)
    decay[...] = jnp.zeros_like(decay)
    loads[0].wait()
    loads[1].wait()
    pl.semaphore_wait(barrier, n_sp + n_tp - 2)
    ring.pump(1)
    for load in loads[2:7]:
        load.wait()

    @pl.loop(0, chunks)
    def _(i):
        here = rows_at(i, CHUNK)
        column_sums, _ = fading_sums(fading[i])
        total_fading = column_sums[CHUNK - 1 :, :]
        later = jnp.exp(total_fading - column_sums)
        for group, (_, keys, switches, kept, before, state, key_width, start) in enumerate(groups):
            mine = slice(start, start + keys.shape[1])
            sums = channel_sums(switches[here, :])
            kept[here, :] = sums
            middle = sums[MIDDLE : MIDDLE + 1, :]
            inverse_keys = (keys[here, :].astype(jnp.float32) * jnp.exp(middle - sums)).astype(jnp.bfloat16)
            keys[here, :] = inverse_keys
            before[i] = (state[...] * jnp.exp(middle)).astype(jnp.bfloat16)
            starts[i, :, mine] = jnp.exp(decay[:1, mine] + middle)
            weighted = (values[group, here, :].astype(jnp.float32) * later).astype(jnp.bfloat16)
            state[...] = advanced(state[...], inverse_keys, weighted, sums, total_fading, key_width)
            decay[:, mine] += sums[CHUNK - 1 :, :] + total_fading

    def pack(slot, first, second, factor):
        packs[slot, :DV, :width_a] = first.astype(jnp.bfloat16)
        packs[slot, :DV, width_a:] = second.astype(jnp.bfloat16)
        packs[slot, DV:, :] = jnp.broadcast_to(factor, (PAD, width)).astype(jnp.bfloat16)

    whole_decay = jnp.exp(decay[:1, :])
    pack(0, state_a[...], state_b[...], whole_decay)
    odd = place % 2
    mate = place + 1 - 2 * odd
    pair = remote(packs.at[0], pair_got, pair_sems.at[0], pair_sems.at[1], (mate, tp_place))
    pair.start()
    pair.wait_recv()
    got = pair_got[...].astype(jnp.float32)
    got_a, got_b, got_decay = got[:DV, :width_a], got[:DV, width_a:], got[DV : DV + 1, :]
    is_odd = odd == 1
    pair_a = jnp.where(
        is_odd,
        whole_decay[:, :width_a] * got_a + state_a[...],
        got_decay[:, :width_a] * state_a[...] + got_a,
    )
    pair_b = jnp.where(
        is_odd,
        whole_decay[:, width_a:] * got_b + state_b[...],
        got_decay[:, width_a:] * state_b[...] + got_b,
    )
    pack(1, pair_a, pair_b, whole_decay * got_decay)
    pairs, pair_place = n_sp // 2, place // 2

    def to_later(k):
        return remote(
            packs.at[1],
            later_got.at[k - 1],
            later_send.at[k - 1],
            later_receive.at[k - 1],
            ((place + 2 * k) % n_sp, tp_place),
        )

    for k in range(1, pairs):

        @pl.when(pair_place + k < pairs)
        def _():
            to_later(k).start()

    ring.pump(4)
    loads[7].wait()
    loads[8].wait()

    row, column = positions()
    causal = column <= row

    @pl.loop(0, chunks)
    def _(i):
        here = rows_at(i, CHUNK)
        column_sums, row_sums = fading_sums(fading[i])
        since_start = jnp.exp(column_sums)
        between = jnp.where(causal, jnp.exp(jnp.minimum(column_sums - row_sums, 0.0)), 0.0)
        for group, (queries, keys, _, kept, before, _, key_width, _) in enumerate(groups):
            sums = kept[here, :]
            middle = sums[MIDDLE : MIDDLE + 1, :]
            spread = queries[here, :].astype(jnp.float32) * (jnp.exp(sums - middle) * key_width**-0.5)
            scaled = spread.astype(jnp.bfloat16)
            queries[here, :] = (spread * since_start).astype(jnp.bfloat16)
            inverse_keys = keys[here, :]
            local = before[i]
            for h in range(keys.shape[1] // key_width):
                if key_width % 128 == 0:
                    mine = slice(h * key_width, (h + 1) * key_width)
                    q, k, s = scaled[:, mine], inverse_keys[:, mine], local[:, mine]
                else:
                    q = jnp.where(lanes_of(h, keys.shape[1], key_width), scaled, jnp.zeros_like(scaled))
                    k, s = inverse_keys, local
                scores = jnp.where(causal, dot(q, k, ((1,), (1,))) * between, 0.0).astype(jnp.bfloat16)
                head = dot(scores, values[group, here, h * DV : (h + 1) * DV], ((1,), (0,)))
                heads[group, here, h * DV : (h + 1) * DV] = head + since_start * dot(q, s, ((1,), (1,)))

    ring.pump(6)
    state_a[...] = jnp.zeros_like(state_a)
    state_b[...] = jnp.zeros_like(state_b)
    for k in range(pairs - 1, 0, -1):

        @pl.when(pair_place >= k)
        def _():
            to_later(k).wait_recv()
            part = later_got[k - 1].astype(jnp.float32)
            factor = part[DV : DV + 1, :]
            state_a[...] = factor[:, :width_a] * state_a[...] + part[:DV, :width_a]
            state_b[...] = factor[:, width_a:] * state_b[...] + part[:DV, width_a:]

    state_a[...] = jnp.where(is_odd, got_decay[:, :width_a] * state_a[...] + got_a, state_a[...])
    state_b[...] = jnp.where(is_odd, got_decay[:, width_a:] * state_b[...] + got_b, state_b[...])
    for load in loads[9:]:
        load.wait()

    def attend(i):
        here = rows_at(i, CHUNK)
        pieces = []
        for group, (queries, _, _, _, _, state, key_width, start) in enumerate(groups):
            key_lanes = queries.shape[1]
            earlier = (state[...] * starts[i, :, start : start + key_lanes]).astype(jnp.bfloat16)
            scaled = queries[here, :]
            for h in range(key_lanes // key_width):
                lanes = slice(h * DV, (h + 1) * DV)
                if key_width % 128 == 0:
                    mine = slice(h * key_width, (h + 1) * key_width)
                    q, s = scaled[:, mine], earlier[:, mine]
                else:
                    q = jnp.where(lanes_of(h, key_lanes, key_width), scaled, jnp.zeros_like(scaled))
                    s = earlier
                head = heads[group, here, lanes] + dot(q, s, ((1,), (1,)))
                inverse = lax.rsqrt(jnp.mean(head * head, axis=-1, keepdims=True) + EPS)
                gate = gates[group, here, lanes].astype(jnp.float32)
                silu = gate / (1.0 + jnp.exp(-gate))
                pieces.append((silu * (head * inverse * gains[group : group + 1, lanes])).astype(jnp.bfloat16))
        return dot(jnp.concatenate(pieces, axis=1), projection[...], ((1,), (0,)))

    def chip_at(k):
        return (chip + 1 + k) % chips

    def terms_copy(slot):
        return remote(
            terms.at[slot], partner_terms.at[slot], terms_send.at[slot], terms_receive.at[slot], partner
        )

    def cross_copy(j, u):
        slot = j * units + u
        return remote(
            cross_terms.at[slot],
            cross_got.at[slot],
            cross_send.at[slot],
            cross_receive.at[slot],
            (place, 2 * chip_at(j) + core),
        )

    @pl.loop(0, chips * units)
    def _(k):
        other, u = chip_at(k // units), k % units
        slot = other * units + u
        terms[slot] = attend((2 * other + 1 - core) * units + u).astype(jnp.bfloat16)
        terms_copy(slot).start()

    @pl.loop(0, (chips - 1) * units)
    def _(k):
        j, u = k // units, k % units
        other = chip_at(j)
        slot = other * units + u
        total = attend((2 * other + core) * units + u)
        terms_copy(slot).wait_recv()
        cross_terms[k] = (total + partner_terms[slot].astype(jnp.float32)).astype(jnp.bfloat16)
        cross_copy(j, u).start()

    @pl.loop(0, units)
    def _(u):
        slot = chip * units + u
        total = attend((2 * chip + core) * units + u)
        terms_copy(slot).wait_recv()
        own_sum[u] = total + partner_terms[slot].astype(jnp.float32)

    ring.pump(8)

    def own_at(owner, u):
        return all_rows.at[rows_at(owner * units + u, CHUNK), :]

    def rows_copy(j, u, owner):
        slot = j * units + u
        ref = own_at(owner, u)
        return remote(
            ref, ref, rows_send.at[slot], rows_receive.at[slot], (place, 2 * chip_at(j) + core)
        )

    def passed_copy(j, u, owner):
        slot = j * units + u
        ref = own_at(owner, u)
        return remote(ref, ref, passed_send.at[slot], passed_receive.at[slot], partner)

    def sender_chip(j):
        return (chip - 1 - j + chips) % chips

    for u in range(units):
        here = slice(u * CHUNK, (u + 1) * CHUNK)
        total = residual[here, :].astype(jnp.float32) + own_sum[u]
        for j in range(chips - 1):
            cross_copy(j, u).wait_recv()
            total = total + cross_got[j * units + u].astype(jnp.float32)
        rounded = total.astype(jnp.bfloat16)
        mid[here, :] = rounded
        widened = rounded.astype(jnp.float32)
        inverse = lax.rsqrt(jnp.mean(widened * widened, axis=-1, keepdims=True) + EPS)
        all_rows[rows_at(tp_place * units + u, CHUNK), :] = (widened * inverse * row_gain[...]).astype(jnp.bfloat16)
        for j in range(chips - 1):
            rows_copy(j, u, tp_place).start()
        passed_copy(chips - 1, u, tp_place).start()
    ring.pump(10)
    for u in range(units):
        for j in range(chips - 1):
            rows_copy(j, u, 2 * sender_chip(j) + core).wait_recv()
            passed_copy(j, u, 2 * sender_chip(j) + core).start()
    for u in range(units):
        for j in range(chips):
            passed_copy(j, u, 2 * sender_chip(j) + 1 - core).wait_recv()
    ring.pump(16)
    ring.arrive_gates()

    ff = hidden.shape[1]
    tile = 256
    tiles = ff // tile

    def first_half(n):
        lanes = rows_at(n, tile)
        everything = all_rows[...]
        gate_sum = dot(everything, gate_full[:, lanes], ((1,), (0,)))
        up_sum = dot(everything, up_full[:, lanes], ((1,), (0,)))
        hidden[:, lanes] = (gate_sum / (1.0 + jnp.exp(-gate_sum)) * up_sum).astype(jnp.bfloat16)

    pl.loop(0, tiles // 2)(first_half)
    ring.pump(17)
    pl.loop(tiles // 2, tiles)(first_half)
    ring.pump(18)

    columns = down_hbm.shape[1]

    def half_copy(b):
        return remote(
            stage.at[b, :, 1 - core], stage_partner.at[b], half_send.at[b], half_receive.at[b], partner
        )

    def last_copy(b, j):
        slot = b * max(chips - 1, 1) + j
        return remote(
            stage_cross.at[slot],
            stage_got.at[slot],
            last_send.at[slot],
            last_receive.at[slot],
            (place, 2 * chip_at(j) + core),
        )

    def multiply(b, origin):
        product = dot(hidden[...], down_full[origin], ((1,), (0,))).astype(jnp.bfloat16)
        stage[b] = product.reshape(chips, 2, own_rows, columns)
        half_copy(b).start()

    def combine(b):
        half_copy(b).wait_recv()
        for j in range(chips - 1):
            other = chip_at(j)
            both = stage[b, other, core].astype(jnp.float32) + stage_partner[b, other].astype(jnp.float32)
            stage_cross[b * max(chips - 1, 1) + j] = both.astype(jnp.bfloat16)
            last_copy(b, j).start()

    def close(b, origin):
        total = stage[b, chip, core].astype(jnp.float32) + stage_partner[b, chip].astype(jnp.float32)
        for j in range(chips - 1):
            last_copy(b, j).wait_recv()
            total = total + stage_got[b * max(chips - 1, 1) + j].astype(jnp.float32)
        down_sum[origin] = total

    blocks = [(0, 0)]
    for hop in range(1, ring.hops + 1):
        blocks += [(way, hop) for way in ((0, 1) if hop <= ring.full else (0,))]
    origins = [ring.origin(way, hop) for way, hop in blocks]
    for b, (way, hop) in enumerate(blocks):
        if hop:
            for side in (0, 1) if hop > ring.full else (way,):
                for piece in ring.carried(side, hop, 2):
                    ring.arrive(side, 1, hop, piece)
        multiply(b, origins[b])
        ring.pump({1: 19, 3: 20, 5: 21}.get(b * 8 // n_sp, 0))
        if b >= 1:
            combine(b - 1)
        if b >= 2:
            close(b - 2, origins[b - 2])
    ring.pump(None)
    combine(len(blocks) - 1)
    if len(blocks) > 1:
        close(len(blocks) - 2, origins[-2])
    close(len(blocks) - 1, origins[-1])

    ring.finish()
    pair.wait_send()
    for k in range(1, pairs):

        @pl.when(pair_place + k < pairs)
        def _():
            to_later(k).wait_send()

    for slot in range(chips * units):
        terms_copy(slot).wait_send()
    for u in range(units):
        for j in range(chips - 1):
            cross_copy(j, u).wait_send()
            rows_copy(j, u, tp_place).wait_send()
        for j in range(chips):
            passed_copy(j, u, tp_place).wait_send()
    for b in range(len(blocks)):
        half_copy(b).wait_send()
        for j in range(chips - 1):
            last_copy(b, j).wait_send()


def per_device(
    residual,
    first_group_queries,
    first_group_keys,
    second_group_queries,
    second_group_keys,
    primary_retain_switch_inputs,
    secondary_retain_switch_inputs,
    timestep_fading_exponent,
    values,
    output_gate_logits,
    head_norm_gains,
    output_projection,
    feedforward_norm_gain,
    gate_projection,
    up_projection,
    down_projection,
):
    n_sp, n_tp = lax.axis_size("sp"), lax.axis_size("tp")
    rows, own_rows = first_group_queries.shape[0], residual.shape[0]
    features = residual.shape[1]
    chunks, units, chips = rows // CHUNK, own_rows // CHUNK, n_tp // 2
    width_a, width_b = first_group_keys.shape[1], second_group_keys.shape[1]
    width = width_a + width_b
    value_width = values.shape[2]
    inner, ff = gate_projection.shape
    columns = down_projection.shape[1]
    hops, crossings = n_sp // 2, max(chips - 1, 1)
    projection = output_projection.reshape(-1, features)
    in_hbm = [
        residual,
        first_group_queries,
        second_group_queries,
        first_group_keys,
        second_group_keys,
        primary_retain_switch_inputs,
        secondary_retain_switch_inputs,
        values,
        output_gate_logits,
        projection,
        gate_projection,
        up_projection,
        down_projection,
    ]
    in_vmem = [
        timestep_fading_exponent.reshape(chunks, 1, CHUNK),
        head_norm_gains,
        feedforward_norm_gain.reshape(1, features),
    ]

    def bf16(*shape):
        return pltpu.VMEM(shape, jnp.bfloat16)

    def f32(*shape):
        return pltpu.VMEM(shape, jnp.float32)

    def sems(*shape):
        return pltpu.SemaphoreType.DMA(shape)

    scratch = [pltpu.VMEM(a.shape, a.dtype) for a in in_hbm[:10]]
    scratch += [bf16(n_sp * inner, ff), bf16(n_sp * inner, ff), bf16(n_sp, ff, columns)]
    scratch += [f32(rows, width_a), f32(rows, width_b)]
    scratch += [bf16(chunks, DV, width_a), bf16(chunks, DV, width_b), f32(chunks, 1, width)]
    scratch += [f32(2, rows, value_width), f32(DV, width_a), f32(DV, width_b), f32(8, width)]
    scratch += [bf16(2, DV + PAD, width), bf16(DV + PAD, width), bf16(max(n_sp // 2 - 1, 1), DV + PAD, width)]
    scratch += [bf16(chips * units, CHUNK, features)] * 2
    scratch += [bf16(crossings * units, CHUNK, features)] * 2
    scratch += [f32(units, CHUNK, features), bf16(rows, features), bf16(rows, ff)]
    scratch += [bf16(n_sp, chips, 2, own_rows, columns), bf16(n_sp, chips, own_rows, columns)]
    scratch += [bf16(n_sp * crossings, own_rows, columns)] * 2
    scratch += [sems(len(in_hbm))]
    scratch += [sems(2, hops, 4), sems(2, hops, 4), sems(2, hops, 2), sems(2, hops, 2)]
    scratch += [sems(2), sems(max(n_sp // 2 - 1, 1)), sems(max(n_sp // 2 - 1, 1))]
    scratch += [sems(chips * units)] * 2
    scratch += [sems(crossings * units)] * 4
    scratch += [sems(chips * units)] * 2
    scratch += [sems(n_sp)] * 2
    scratch += [sems(n_sp * crossings)] * 2
    mid, down_sum = pl.pallas_call(
        functools.partial(layer_kernel, n_sp, n_tp),
        in_specs=[pl.BlockSpec(memory_space=pl.ANY)] * len(in_hbm)
        + [pl.BlockSpec(memory_space=pltpu.VMEM)] * len(in_vmem),
        out_specs=[pl.BlockSpec(memory_space=pltpu.VMEM)] * 2,
        out_shape=[
            jax.ShapeDtypeStruct((own_rows, features), jnp.bfloat16),
            jax.ShapeDtypeStruct((n_sp, own_rows, columns), jnp.float32),
        ],
        scratch_shapes=scratch,
        compiler_params=pltpu.CompilerParams(
            collective_id=0, has_side_effects=True, vmem_limit_bytes=VMEM_BYTES
        ),
        name="layer",
    )(*in_hbm, *in_vmem)
    added = down_sum.transpose(1, 0, 2).reshape(own_rows, features)
    return (mid.astype(jnp.float32) + added).astype(jnp.bfloat16)


def solution(mesh):
    return jax.shard_map(
        per_device,
        mesh=mesh,
        in_specs=(
            P(("sp", "tp"), None),
            P("sp", "tp"),
            P("sp", "tp"),
            P("sp", "tp"),
            P("sp", "tp"),
            P("sp", "tp"),
            P("sp", "tp"),
            P("sp"),
            P(None, "sp", "tp"),
            P(None, "sp", "tp"),
            P(None, "tp"),
            P(None, "tp", None),
            P(),
            P("sp", "tp"),
            P("sp", "tp"),
            P("tp", "sp"),
        ),
        out_specs=P(("sp", "tp"), None),
        check_vma=False,
    )
```

profile of v0, /device:TPU:0, one launch (start us, length us, event | category | flops | bytes accessed | tf_op | source)
XLA Modules:
  0.0 215.7 jit_solution(3776370303179926548)
XLA Ops:
  0.0 209.5 %layer.1 = (bf16[256,2048]{1,0:T(8,128)(2,1)}, f32[8,256,256]{2,1,0:T(8,128)}) custom-call(bf16[256,2048]{1,0:T(8,128)(2,1)} %residual_hbm.1, bf16[1024,256]{1,0:T(8,128)(2,1)} %qa_hbm.1, bf16[1024,128]{1,0:T(8,128)(2,1)} %qb_hbm.1, bf16[1024,256]{1,0:T(8,128)(2,1)} %ka_hbm.1, bf16[1024,128]{1,0:T(8,128)(2,1)} %kb_hbm.1, bf16[1024,256]{1,0:T(8,128)(2,1)} %sa_hbm.1, ...), custom_call_target="tpu_custom_call" | custom-call | tf_op jit(solution)/shard_map/layer/pallas_call | solution.py:696
  209.5 2.9 %copy.17 = f32[256,8,256]{0,2,1:T(8,128)} copy(f32[256,8,256]{2,0,1:T(8,128)} %bitcast.6) | data formatting | bytes 4194304 | tf_op jit(solution)/shard_map/transpose | solution.py:711
  212.4 0.0 copy-start
  212.4 2.0 copy.18
  214.4 0.0 copy-done
  214.4 1.3 add_convert_fusion
Async XLA Ops:
  212.4 2.0 copy-start
where the time goes:
time: 216 us
  Pallas kernels  209 us (97%)
  local copies, waits for them, and re-layouts  4.91 us (2%)
    pallas_call x1, Pallas kernels, per_device(): pl.pallas_call(functools.partial(layer_kernel, n_sp, n_tp), in_specs=[pl....  209 us

commit v1 on v0

--- a/solution.py
+++ b/solution.py
@@ -18,6 +18,7 @@
 EPS = 1e-06
 SOFTNESS_SCALE = 16.0
 VMEM_BYTES = 66_000_000
+DEPTH = 4
 
 def dot(a, b, dims):
     return lax.dot_general(a, b, (dims, ((), ())), preferred_element_type=jnp.float32)
@@ -91,71 +92,112 @@
     return pl.ds(pl.multiple_of(index * count, count), count)
 
 
-class Ring:
-    def __init__(self, peers, place, tp_place, gate, up, down, gate_sems, down_sems):
-        self.peers, self.tp_place = peers, tp_place
-        self.gate, self.up, self.down = gate, up, down
-        self.gate_sems, self.down_sems = gate_sems, down_sems
-        self.position = jnp.where(place % 2 == 0, place // 2, peers - 1 - place // 2)
-        self.full = (peers - 1) // 2
-        self.hops = peers // 2
-        self.beyond = (self.origin(0, -1), self.origin(1, -1))
+class Line:
+    def __init__(self, pairs, place, tp_place, whole, shards, sems, mate_sems):
+        self.pairs, self.place, self.tp_place = pairs, place, tp_place
+        self.pair, self.side = place // 2, place % 2
+        self.gate, self.up, self.down = whole
+        self.shards = shards
+        self.sems, self.mate_sems = sems, mate_sems
+        self.inner, self.half = shards[0].shape[0], shards[2].shape[0] // 2
         self.waited = set()
         self.issued = 0
-        self.events = ([], [])
-        for way in (0, 1):
-            for matrix, count in ((0, 4), (1, 2)):
-                for hop in range(1, self.hops + 1):
-                    for piece in self.carried(way, hop, count):
-                        self.events[way].append((matrix, hop, piece))
-
-    def origin(self, way, distance):
-        place = (self.position + (distance if way else -distance) + 2 * self.peers) % self.peers
-        return jnp.where(place < (self.peers + 1) // 2, 2 * place, 2 * (self.peers - 1 - place) + 1)
-
-    def carried(self, way, hop, count):
-        if hop <= self.full:
-            return range(count)
-        return range(count // 2, count) if way else range(count // 2)
-
-    def piece(self, matrix, origin, piece):
+        self.events = [
+            (matrix, hop, piece)
+            for matrix, count in ((0, 4), (1, 2))
+            for hop in range(1, pairs)
+            for piece in range(count)
+        ]
+
+    def shard(self, kind, side):
+        half = rows_at(side, self.half)
+        return self.shards[kind].at[half, :] if kind == 2 else self.shards[kind].at[:, half]
+
+    def landing(self, kind, origin):
+        if kind == 2:
+            return self.down.at[origin]
+        return (self.up if kind else self.gate).at[rows_at(origin, self.inner), :]
+
+    def own(self, kind):
+        return self.shard(kind, self.side), self.landing(kind, self.place)
+
+    def mate_copy(self, kind):
+        return remote(
+            self.shard(kind, 1 - self.side),
+            self.landing(kind, self.place),
+            self.mate_sems[0].at[kind],
+            self.mate_sems[1].at[kind],
+            (self.place + 1 - 2 * self.side, self.tp_place),
+        )
+
+    def arrive_mate(self, kind):
+        if ("mate", kind) not in self.waited:
+            self.waited.add(("mate", kind))
+            self.mate_copy(kind).wait_recv()
+
+    def reaches(self, way, distance):
+        return self.pair + distance < self.pairs if way else self.pair >= distance
+
+    def copy(self, way, matrix, hop, piece, distance):
+        pair = (self.pair + (distance if way else -distance) + self.pairs) % self.pairs
         if matrix:
-            half = self.down.shape[1] // 2
-            return self.down.at[origin, pl.ds(piece * half, half), :]
-        half = self.gate.shape[0] // self.peers // 2
-        return (self.up if piece // 2 else self.gate).at[rows_at(origin * 2 + piece % 2, half), :]
-
-    def copy(self, way, matrix, hop, piece, distance):
-        ref = self.piece(matrix, self.origin(way, distance), piece)
-        send, receive = self.down_sems if matrix else self.gate_sems
+            ref = self.landing(2, 2 * pair + piece)
+        else:
+            ref = self.landing(piece % 2, 2 * pair + (self.side if piece < 2 else 1 - self.side))
+        send, receive = self.sems[matrix]
         at = (way, hop - 1, piece)
-        return remote(ref, ref, send.at[at], receive.at[at], (self.beyond[way], self.tp_place))
+        beyond = (self.place + (-2 if way else 2) + 2 * self.pairs) % (2 * self.pairs)
+        return remote(ref, ref, send.at[at], receive.at[at], (beyond, self.tp_place))
 
     def arrive(self, way, matrix, hop, piece):
         if (way, matrix, hop, piece) not in self.waited:
             self.waited.add((way, matrix, hop, piece))
-            self.copy(way, matrix, hop, piece, hop).wait_recv()
+
+            @pl.when(self.reaches(way, hop))
+            def _():
+                self.copy(way, matrix, hop, piece, hop).wait_recv()
+
+    def passes(self, way, hop):
+        return self.reaches(way, hop - 1) & self.reaches(1 - way, 1)
 
     def pump(self, until):
-        until = len(self.events[0]) if until is None else (until * len(self.events[0]) + 20) // 21
+        until = len(self.events) if until is None else (until * len(self.events) + 17) // 18
         while self.issued < until:
+            matrix, hop, piece = self.events[self.issued]
+            if hop == 1 and (matrix or piece >= 2):
+                self.arrive_mate(2 if matrix else piece % 2)
             for way in (0, 1):
-                matrix, hop, piece = self.events[way][self.issued]
                 if hop > 1:
                     self.arrive(way, matrix, hop - 1, piece)
-                self.copy(way, matrix, hop, piece, hop - 1).start()
+
+                @pl.when(self.passes(way, hop))
+                def _():
+                    self.copy(way, matrix, hop, piece, hop - 1).start()
+
             self.issued += 1
 
     def arrive_gates(self):
-        for hop in range(1, self.hops + 1):
+        for hop in range(1, self.pairs):
+            for piece in range(4):
+                for way in (0, 1):
+                    self.arrive(way, 0, hop, piece)
+
+    def nth(self, q):
+        low, high = self.pair, self.pairs - 1 - self.pair
+        both = jnp.minimum(low, high)
+        near = self.pair + ((q // 2) if q % 2 == 0 else -((q + 1) // 2))
+        far = jnp.where(low > high, self.pair - (q - both), self.pair + (q - both))
+        return jnp.where(q <= 2 * both, near, far)
+
+    def finish(self):
+        for kind in range(3):
+            self.mate_copy(kind).wait_send()
+        for matrix, hop, piece in self.events:
             for way in (0, 1):
-                for piece in self.carried(way, hop, 4):
-                    self.arrive(way, 0, hop, piece)
-
-    def finish(self):
-        for way in (0, 1):
-            for matrix, hop, piece in self.events[way]:
-                self.copy(way, matrix, hop, piece, hop - 1).wait_send()
+
+                @pl.when(self.passes(way, hop))
+                def _():
+                    self.copy(way, matrix, hop, piece, hop - 1).wait_send()
 
 
 def layer_kernel(
@@ -177,8 +219,43 @@
     fading,
     gains,
     row_gain,
-    mid,
-    down_sum,
+    *others,
+):
+    outs, scratch = (others[:1], others[1:]) if down_hbm.shape[1] % 128 == 0 else (others[:2], others[2:])
+    layer_body(
+        n_sp,
+        n_tp,
+        (
+            residual_hbm,
+            qa_hbm,
+            qb_hbm,
+            ka_hbm,
+            kb_hbm,
+            sa_hbm,
+            sb_hbm,
+            values_hbm,
+            gates_hbm,
+            projection_hbm,
+            gate_hbm,
+            up_hbm,
+            down_hbm,
+        ),
+        fading,
+        gains,
+        row_gain,
+        outs,
+        *scratch,
+    )
+
+
+def layer_body(
+    n_sp,
+    n_tp,
+    in_hbm,
+    fading,
+    gains,
+    row_gain,
+    outs,
     residual,
     qa,
     qb,
@@ -215,7 +292,11 @@
     stage_partner,
     stage_cross,
     stage_got,
+    mid,
+    result,
     load_sems,
+    mate_send,
+    mate_receive,
     gate_send,
     gate_receive,
     down_send,
@@ -235,7 +316,10 @@
     half_receive,
     last_send,
     last_receive,
+    out_sems,
 ):
+    residual_hbm, qa_hbm, qb_hbm, ka_hbm, kb_hbm, sa_hbm, sb_hbm, values_hbm, gates_hbm, projection_hbm = in_hbm[:10]
+    shards = in_hbm[10:]
     place, tp_place = lax.axis_index("sp"), lax.axis_index("tp")
     chip, core = tp_place // 2, tp_place % 2
     chips = n_tp // 2
@@ -248,7 +332,18 @@
         (qa, ka, sa, sums_a, before_a, state_a, FIRST_KEY_SIZE, 0),
         (qb, kb, sb, sums_b, before_b, state_b, SECOND_KEY_SIZE, width_a),
     )
-    inner = gate_hbm.shape[0]
+    odd = place % 2
+    mate = place + 1 - 2 * odd
+    pairs, pair_place = n_sp // 2, place // 2
+    line = Line(
+        pairs,
+        place,
+        tp_place,
+        (gate_full, up_full, down_full),
+        shards,
+        ((gate_send, gate_receive), (down_send, down_receive)),
+        (mate_send, mate_receive),
+    )
 
     barrier = pltpu.get_barrier_semaphore()
     for k in range(1, n_sp):
@@ -260,9 +355,17 @@
             barrier, inc=1, device_id=(place, (tp_place + k) % n_tp), device_id_type=MESH
         )
 
+    for k in range(1, chips):
+        pl.semaphore_signal(
+            barrier,
+            inc=1,
+            device_id=(mate, 2 * ((chip + k) % chips) + core),
+            device_id_type=MESH,
+        )
+
     loads = [
-        (gate_hbm, gate_full.at[rows_at(place, inner), :]),
-        (up_hbm, up_full.at[rows_at(place, inner), :]),
+        line.own(0),
+        line.own(1),
         (ka_hbm, ka),
         (kb_hbm, kb),
         (sa_hbm, sa),
@@ -270,7 +373,7 @@
         (values_hbm, values),
         (qa_hbm, qa),
         (qb_hbm, qb),
-        (down_hbm, down_full.at[place]),
+        line.own(2),
         (projection_hbm, projection),
         (gates_hbm, gates),
         (residual_hbm, residual),
@@ -278,23 +381,14 @@
     loads = [pltpu.make_async_copy(a, b, load_sems.at[i]) for i, (a, b) in enumerate(loads)]
     for load in loads:
         load.start()
-    ring = Ring(
-        n_sp,
-        place,
-        tp_place,
-        gate_full,
-        up_full,
-        down_full,
-        (gate_send, gate_receive),
-        (down_send, down_receive),
-    )
     state_a[...] = jnp.zeros_like(state_a)
     state_b[...] = jnp.zeros_like(state_b)
     decay[...] = jnp.zeros_like(decay)
     loads[0].wait()
     loads[1].wait()
-    pl.semaphore_wait(barrier, n_sp + n_tp - 2)
-    ring.pump(1)
+    pl.semaphore_wait(barrier, n_sp + n_tp + chips - 3)
+    line.mate_copy(0).start()
+    line.pump(1)
     for load in loads[2:7]:
         load.wait()
 
@@ -324,10 +418,9 @@
 
     whole_decay = jnp.exp(decay[:1, :])
     pack(0, state_a[...], state_b[...], whole_decay)
-    odd = place % 2
-    mate = place + 1 - 2 * odd
     pair = remote(packs.at[0], pair_got, pair_sems.at[0], pair_sems.at[1], (mate, tp_place))
     pair.start()
+    line.mate_copy(1).start()
     pair.wait_recv()
     got = pair_got[...].astype(jnp.float32)
     got_a, got_b, got_decay = got[:DV, :width_a], got[:DV, width_a:], got[DV : DV + 1, :]
@@ -343,7 +436,6 @@
         got_decay[:, width_a:] * state_b[...] + got_b,
     )
     pack(1, pair_a, pair_b, whole_decay * got_decay)
-    pairs, pair_place = n_sp // 2, place // 2
 
     def to_later(k):
         return remote(
@@ -360,7 +452,9 @@
         def _():
             to_later(k).start()
 
-    ring.pump(4)
+    line.mate_copy(2).start()
+    loads[9].wait()
+    line.pump(3)
     loads[7].wait()
     loads[8].wait()
 
@@ -392,7 +486,6 @@
                 head = dot(scores, values[group, here, h * DV : (h + 1) * DV], ((1,), (0,)))
                 heads[group, here, h * DV : (h + 1) * DV] = head + since_start * dot(q, s, ((1,), (1,)))
 
-    ring.pump(6)
     state_a[...] = jnp.zeros_like(state_a)
     state_b[...] = jnp.zeros_like(state_b)
     for k in range(pairs - 1, 0, -1):
@@ -407,7 +500,7 @@
 
     state_a[...] = jnp.where(is_odd, got_decay[:, :width_a] * state_a[...] + got_a, state_a[...])
     state_b[...] = jnp.where(is_odd, got_decay[:, width_a:] * state_b[...] + got_b, state_b[...])
-    for load in loads[9:]:
+    for load in loads[10:]:
         load.wait()
 
     def attend(i):
@@ -474,26 +567,31 @@
         terms_copy(slot).wait_recv()
         own_sum[u] = total + partner_terms[slot].astype(jnp.float32)
 
-    ring.pump(8)
+    line.pump(6)
+
+    peers = [(dy, dx) for dy in (0, 1) for dx in range(chips) if dy or dx]
+
+    def device_at(dy, dx):
+        return (mate if dy else place, 2 * ((chip + dx) % chips) + core)
+
+    def owner_at(dy, dx, of_core):
+        side = 1 - odd if dy else odd
+        return side * n_tp + 2 * ((chip - dx + chips) % chips) + of_core
 
     def own_at(owner, u):
         return all_rows.at[rows_at(owner * units + u, CHUNK), :]
 
-    def rows_copy(j, u, owner):
-        slot = j * units + u
+    def rows_copy(k, u, owner):
+        slot = k * units + u
         ref = own_at(owner, u)
-        return remote(
-            ref, ref, rows_send.at[slot], rows_receive.at[slot], (place, 2 * chip_at(j) + core)
-        )
-
-    def passed_copy(j, u, owner):
-        slot = j * units + u
+        return remote(ref, ref, rows_send.at[slot], rows_receive.at[slot], device_at(*peers[k]))
+
+    def passed_copy(k, u, owner):
+        slot = k * units + u
         ref = own_at(owner, u)
         return remote(ref, ref, passed_send.at[slot], passed_receive.at[slot], partner)
 
-    def sender_chip(j):
-        return (chip - 1 - j + chips) % chips
-
+    mine = owner_at(0, 0, core)
     for u in range(units):
         here = slice(u * CHUNK, (u + 1) * CHUNK)
         total = residual[here, :].astype(jnp.float32) + own_sum[u]
@@ -504,96 +602,117 @@
         mid[here, :] = rounded
         widened = rounded.astype(jnp.float32)
         inverse = lax.rsqrt(jnp.mean(widened * widened, axis=-1, keepdims=True) + EPS)
-        all_rows[rows_at(tp_place * units + u, CHUNK), :] = (widened * inverse * row_gain[...]).astype(jnp.bfloat16)
-        for j in range(chips - 1):
-            rows_copy(j, u, tp_place).start()
-        passed_copy(chips - 1, u, tp_place).start()
-    ring.pump(10)
+        all_rows[rows_at(mine * units + u, CHUNK), :] = (widened * inverse * row_gain[...]).astype(jnp.bfloat16)
+        for k in range(len(peers)):
+            rows_copy(k, u, mine).start()
+        passed_copy(len(peers), u, mine).start()
+    line.pump(8)
     for u in range(units):
-        for j in range(chips - 1):
-            rows_copy(j, u, 2 * sender_chip(j) + core).wait_recv()
-            passed_copy(j, u, 2 * sender_chip(j) + core).start()
+        for k, peer in enumerate(peers):
+            rows_copy(k, u, owner_at(*peer, core)).wait_recv()
+            passed_copy(k, u, owner_at(*peer, core)).start()
+        line.pump(10 + 2 * u)
     for u in range(units):
-        for j in range(chips):
-            passed_copy(j, u, 2 * sender_chip(j) + 1 - core).wait_recv()
-    ring.pump(16)
-    ring.arrive_gates()
-
+        for k, peer in enumerate(peers + [(0, 0)]):
+            passed_copy(k, u, owner_at(*peer, 1 - core)).wait_recv()
+    line.pump(14)
+    line.arrive_gates()
     ff = hidden.shape[1]
-    tile = 256
+    tile = 256 if ff % 256 == 0 else 128
     tiles = ff // tile
+    bands = 2 * chips
+    band = 2 * own_rows
 
     def first_half(n):
-        lanes = rows_at(n, tile)
-        everything = all_rows[...]
-        gate_sum = dot(everything, gate_full[:, lanes], ((1,), (0,)))
-        up_sum = dot(everything, up_full[:, lanes], ((1,), (0,)))
-        hidden[:, lanes] = (gate_sum / (1.0 + jnp.exp(-gate_sum)) * up_sum).astype(jnp.bfloat16)
-
-    pl.loop(0, tiles // 2)(first_half)
-    ring.pump(17)
-    pl.loop(tiles // 2, tiles)(first_half)
-    ring.pump(18)
-
-    columns = down_hbm.shape[1]
+        lanes = rows_at(n // bands, tile)
+        here = rows_at(n % bands, band)
+        gate_sum = dot(all_rows[here, :], gate_full[:, lanes], ((1,), (0,)))
+        up_sum = dot(all_rows[here, :], up_full[:, lanes], ((1,), (0,)))
+        hidden[here, lanes] = (gate_sum / (1.0 + jnp.exp(-gate_sum)) * up_sum).astype(jnp.bfloat16)
+
+    pl.loop(0, tiles * bands * 2 // 3)(first_half)
+    line.pump(15)
+    pl.loop(tiles * bands * 2 // 3, tiles * bands)(first_half)
+
+    columns = shards[2].shape[1]
+    direct = columns % 128 == 0
+    count = len(peers)
 
     def half_copy(b):
         return remote(
-            stage.at[b, :, 1 - core], stage_partner.at[b], half_send.at[b], half_receive.at[b], partner
-        )
-
-    def last_copy(b, j):
-        slot = b * max(chips - 1, 1) + j
+            stage.at[b % DEPTH, :, 1 - core], stage_partner.at[b], half_send.at[b], half_receive.at[b], partner
+        )
+
+    def last_copy(b, k):
+        slot = b * count + k
         return remote(
-            stage_cross.at[slot],
+            stage_cross.at[b % DEPTH * count + k],
             stage_got.at[slot],
             last_send.at[slot],
             last_receive.at[slot],
-            (place, 2 * chip_at(j) + core),
-        )
+            device_at(*peers[k]),
+        )
+
+    def out_copy(b, origin):
+        lanes = rows_at(origin, columns)
+        done = (mid.at[:, lanes], outs[0].at[:, lanes]) if direct else (result.at[b], outs[1].at[origin])
+        return pltpu.make_async_copy(*done, out_sems.at[b])
 
     def multiply(b, origin):
-        product = dot(hidden[...], down_full[origin], ((1,), (0,))).astype(jnp.bfloat16)
-        stage[b] = product.reshape(chips, 2, own_rows, columns)
+        if b >= DEPTH:
+            half_copy(b - DEPTH).wait_send()
+
+        @pl.loop(0, bands)
+        def _(g):
+            product = dot(hidden[rows_at(g, band), :], down_full[origin], ((1,), (0,))).astype(jnp.bfloat16)
+            stage[b % DEPTH, g] = product.reshape(2, own_rows, columns)
+
         half_copy(b).start()
 
     def combine(b):
         half_copy(b).wait_recv()
-        for j in range(chips - 1):
-            other = chip_at(j)
-            both = stage[b, other, core].astype(jnp.float32) + stage_partner[b, other].astype(jnp.float32)
-            stage_cross[b * max(chips - 1, 1) + j] = both.astype(jnp.bfloat16)
-            last_copy(b, j).start()
+        for k, (dy, dx) in enumerate(peers):
+            if b >= DEPTH:
+                last_copy(b - DEPTH, k).wait_send()
+            band_at = (1 - odd if dy else odd) * chips + (chip + dx) % chips
+            both = stage[b % DEPTH, band_at, core].astype(jnp.float32) + stage_partner[b, band_at].astype(jnp.float32)
+            stage_cross[b % DEPTH * count + k] = both.astype(jnp.bfloat16)
+            last_copy(b, k).start()
 
     def close(b, origin):
-        total = stage[b, chip, core].astype(jnp.float32) + stage_partner[b, chip].astype(jnp.float32)
-        for j in range(chips - 1):
-            last_copy(b, j).wait_recv()
-            total = total + stage_got[b * max(chips - 1, 1) + j].astype(jnp.float32)
-        down_sum[origin] = total
-
-    blocks = [(0, 0)]
-    for hop in range(1, ring.hops + 1):
-        blocks += [(way, hop) for way in ((0, 1) if hop <= ring.full else (0,))]
-    origins = [ring.origin(way, hop) for way, hop in blocks]
-    for b, (way, hop) in enumerate(blocks):
-        if hop:
-            for side in (0, 1) if hop > ring.full else (way,):
-                for piece in ring.carried(side, hop, 2):
-                    ring.arrive(side, 1, hop, piece)
+        band_at = odd * chips + chip
+        total = stage[b % DEPTH, band_at, core].astype(jnp.float32) + stage_partner[b, band_at].astype(jnp.float32)
+        for k in range(count):
+            last_copy(b, k).wait_recv()
+            total = total + stage_got[b * count + k].astype(jnp.float32)
+        if direct:
+            lanes = rows_at(origin, columns)
+            mid[:, lanes] = (mid[:, lanes].astype(jnp.float32) + total).astype(jnp.bfloat16)
+        else:
+            result[b] = total
+        out_copy(b, origin).start()
+
+    origins = [2 * line.nth(b // 2) + b % 2 for b in range(n_sp)]
+    for b in range(n_sp):
+        if b >= 2:
+            line.arrive(0, 1, b // 2, b % 2)
+            line.arrive(1, 1, b // 2, b % 2)
         multiply(b, origins[b])
-        ring.pump({1: 19, 3: 20, 5: 21}.get(b * 8 // n_sp, 0))
         if b >= 1:
             combine(b - 1)
-        if b >= 2:
-            close(b - 2, origins[b - 2])
-    ring.pump(None)
-    combine(len(blocks) - 1)
-    if len(blocks) > 1:
-        close(len(blocks) - 2, origins[-2])
-    close(len(blocks) - 1, origins[-1])
-
-    ring.finish()
+        line.pump({1: 16, 3: 17, 4: 18}.get(b * 8 // n_sp, 0))
+        if b >= 3:
+            close(b - 3, origins[b - 3])
+    line.pump(None)
+    combine(n_sp - 1)
+    for b in range(max(n_sp - 3, 0), n_sp):
+        close(b, origins[b])
+    for b in range(n_sp):
+        out_copy(b, origins[b]).wait()
+    if not direct:
+        pltpu.sync_copy(mid, outs[0])
+
+    line.finish()
     pair.wait_send()
     for k in range(1, pairs):
 
@@ -606,13 +725,14 @@
     for u in range(units):
         for j in range(chips - 1):
             cross_copy(j, u).wait_send()
-            rows_copy(j, u, tp_place).wait_send()
-        for j in range(chips):
-            passed_copy(j, u, tp_place).wait_send()
-    for b in range(len(blocks)):
+        for k in range(count):
+            rows_copy(k, u, mine).wait_send()
+        for k in range(count + 1):
+            passed_copy(k, u, mine).wait_send()
+    for b in range(max(n_sp - DEPTH, 0), n_sp):
         half_copy(b).wait_send()
-        for j in range(chips - 1):
-            last_copy(b, j).wait_send()
+        for k in range(count):
+            last_copy(b, k).wait_send()
 
 
 def per_device(
@@ -642,7 +762,8 @@
     value_width = values.shape[2]
     inner, ff = gate_projection.shape
     columns = down_projection.shape[1]
-    hops, crossings = n_sp // 2, max(chips - 1, 1)
+    pairs, crossings, peers = n_sp // 2, max(chips - 1, 1), 2 * chips - 1
+    direct = columns % 128 == 0
     projection = output_projection.reshape(-1, features)
     in_hbm = [
         residual,
@@ -675,41 +796,46 @@
         return pltpu.SemaphoreType.DMA(shape)
 
     scratch = [pltpu.VMEM(a.shape, a.dtype) for a in in_hbm[:10]]
-    scratch += [bf16(n_sp * inner, ff), bf16(n_sp * inner, ff), bf16(n_sp, ff, columns)]
+    scratch += [bf16(n_sp * inner, ff // 2)] * 2 + [bf16(n_sp, ff // 2, columns)]
     scratch += [f32(rows, width_a), f32(rows, width_b)]
     scratch += [bf16(chunks, DV, width_a), bf16(chunks, DV, width_b), f32(chunks, 1, width)]
     scratch += [f32(2, rows, value_width), f32(DV, width_a), f32(DV, width_b), f32(8, width)]
     scratch += [bf16(2, DV + PAD, width), bf16(DV + PAD, width), bf16(max(n_sp // 2 - 1, 1), DV + PAD, width)]
     scratch += [bf16(chips * units, CHUNK, features)] * 2
     scratch += [bf16(crossings * units, CHUNK, features)] * 2
-    scratch += [f32(units, CHUNK, features), bf16(rows, features), bf16(rows, ff)]
-    scratch += [bf16(n_sp, chips, 2, own_rows, columns), bf16(n_sp, chips, own_rows, columns)]
-    scratch += [bf16(n_sp * crossings, own_rows, columns)] * 2
-    scratch += [sems(len(in_hbm))]
-    scratch += [sems(2, hops, 4), sems(2, hops, 4), sems(2, hops, 2), sems(2, hops, 2)]
+    scratch += [f32(units, CHUNK, features), bf16(2 * rows, features), bf16(2 * rows, ff // 2)]
+    scratch += [bf16(DEPTH, 2 * chips, 2, own_rows, columns), bf16(n_sp, 2 * chips, own_rows, columns)]
+    scratch += [bf16(DEPTH * peers, own_rows, columns), bf16(n_sp * peers, own_rows, columns)]
+    scratch += [bf16(own_rows, features), f32(*((8, 128) if direct else (n_sp, own_rows, columns)))]
+    scratch += [sems(len(in_hbm)), sems(3), sems(3)]
+    scratch += [sems(2, max(pairs - 1, 1), 4)] * 2 + [sems(2, max(pairs - 1, 1), 2)] * 2
     scratch += [sems(2), sems(max(n_sp // 2 - 1, 1)), sems(max(n_sp // 2 - 1, 1))]
     scratch += [sems(chips * units)] * 2
-    scratch += [sems(crossings * units)] * 4
-    scratch += [sems(chips * units)] * 2
+    scratch += [sems(crossings * units)] * 2
+    scratch += [sems(peers * units)] * 2
+    scratch += [sems((peers + 1) * units)] * 2
     scratch += [sems(n_sp)] * 2
-    scratch += [sems(n_sp * crossings)] * 2
-    mid, down_sum = pl.pallas_call(
+    scratch += [sems(n_sp * peers)] * 2
+    scratch += [sems(n_sp)]
+    row_shape = jax.ShapeDtypeStruct((own_rows, features), jnp.bfloat16)
+    sums_shape = jax.ShapeDtypeStruct((n_sp, own_rows, columns), jnp.float32)
+    outs = [row_shape] if direct else [row_shape, sums_shape]
+    outs = pl.pallas_call(
         functools.partial(layer_kernel, n_sp, n_tp),
         in_specs=[pl.BlockSpec(memory_space=pl.ANY)] * len(in_hbm)
         + [pl.BlockSpec(memory_space=pltpu.VMEM)] * len(in_vmem),
-        out_specs=[pl.BlockSpec(memory_space=pltpu.VMEM)] * 2,
-        out_shape=[
-            jax.ShapeDtypeStruct((own_rows, features), jnp.bfloat16),
-            jax.ShapeDtypeStruct((n_sp, own_rows, columns), jnp.float32),
-        ],
+        out_specs=[pl.BlockSpec(memory_space=pl.ANY)] * len(outs),
+        out_shape=outs,
         scratch_shapes=scratch,
         compiler_params=pltpu.CompilerParams(
             collective_id=0, has_side_effects=True, vmem_limit_bytes=VMEM_BYTES
         ),
         name="layer",
     )(*in_hbm, *in_vmem)
-    added = down_sum.transpose(1, 0, 2).reshape(own_rows, features)
-    return (mid.astype(jnp.float32) + added).astype(jnp.bfloat16)
+    if direct:
+        return outs[0]
+    added = outs[1].transpose(1, 0, 2).reshape(own_rows, features)
+    return (outs[0].astype(jnp.float32) + added).astype(jnp.bfloat16)
 
 
 def solution(mesh):

time: 216 us -> 189 us (0.88)
  Pallas kernels: 209 us -> 186 us
  local copies, waits for them, and re-layouts: 4.91 us -> 2.3 us
    pallas_call x1, Pallas kernels: 209 us -> 186 us  [per_device(): pl.pallas_call(functools.partial(layer_kernel, n_sp, n_tp), in_specs=[pl....]
    transpose x1 -> x0, local copies, waits for them, and re-layouts: 2.89 us -> none  [per_device(): added = down_sum.transpose(1, 0, 2).reshape(own_rows, features)]
    unnamed x2 -> x1, local copies, waits for them, and re-layouts: 0.01 us -> 2.3 us
where the time goes in v1:
time: 189 us
  Pallas kernels  186 us (98%)
  local copies, waits for them, and re-layouts  2.3 us (1%)
    pallas_call x1, Pallas kernels, per_device(): pl.pallas_call(functools.partial(layer_kernel, n_sp, n_tp), in_specs=[pl....  186 us

profile of v1, /device:TPU:0, one launch (start us, length us, event | category | flops | bytes accessed | tf_op | source)
XLA Modules:
  0.0 188.6 jit_solution(10750632474047547218)
XLA Ops:
  0.0 186.3 %layer.1 = bf16[256,2048]{1,0:T(8,128)(2,1)} custom-call(bf16[256,2048]{1,0:T(8,128)(2,1)} %residual_hbm.1, bf16[1024,256]{1,0:T(8,128)(2,1)} %qa_hbm.1, bf16[1024,128]{1,0:T(8,128)(2,1)} %qb_hbm.1, bf16[1024,256]{1,0:T(8,128)(2,1)} %ka_hbm.1, bf16[1024,128]{1,0:T(8,128)(2,1)} %kb_hbm.1, bf16[1024,256]{1,0:T(8,128)(2,1)} %sa_hbm.1, ...), custom_call_target="tpu_custom_call" | custom-call | tf_op jit(solution)/shard_map/layer/pallas_call | solution.py:823
  186.3 2.3 %copy.18 = bf16[256,2048]{1,0:T(8,128)(2,1)} copy(bf16[256,2048]{1,0:T(8,128)(2,1)} %layer.1) | data formatting | bytes 2097152

commit v2 on v1

v2 whole, which is shorter than its diff:
```python
import functools

import jax
import jax.numpy as jnp
from jax import lax
from jax.experimental import pallas as pl
from jax.experimental.pallas import tpu as pltpu
from jax.sharding import PartitionSpec as P

FIRST_KEY_SIZE = 128
SECOND_KEY_SIZE = 64
DV = 128
CHUNK = 128
MIDDLE = CHUNK // 2 - 1
PAD = 16
MESH = pl.DeviceIdType.MESH

EPS = 1e-06
SOFTNESS_SCALE = 16.0
VMEM_BYTES = 62_000_000
DEPTH = 4
EARLY = (1,)

def dot(a, b, dims):
    return lax.dot_general(a, b, (dims, ((), ())), preferred_element_type=jnp.float32)


def positions():
    row = lax.broadcasted_iota(jnp.int32, (CHUNK, CHUNK), 0)
    column = lax.broadcasted_iota(jnp.int32, (CHUNK, CHUNK), 1)
    return row, column


def fading_sums(fading_row):
    row, column = positions()
    as_column = jnp.sum(jnp.where(row == column, fading_row, 0.0), axis=1, keepdims=True)
    column_sums = jnp.sum(jnp.where(column <= row, fading_row, 0.0), axis=1, keepdims=True)
    row_sums = jnp.sum(jnp.where(row <= column, as_column, 0.0), axis=0, keepdims=True)
    return column_sums, row_sums


def channel_sums(switches):
    row, column = positions()
    x = switches.astype(jnp.float32)
    logs = (jnp.minimum(x, 0.0) - jnp.log1p(jnp.exp(-jnp.abs(x)))) * (1.0 / SOFTNESS_SCALE)
    lower = (column <= row).astype(jnp.bfloat16)
    high = logs.astype(jnp.bfloat16)
    low = (logs - high.astype(jnp.float32)).astype(jnp.bfloat16)
    return dot(lower, high, ((1,), (0,))) + dot(lower, low, ((1,), (0,)))


def lanes_of(head, width, key_width):
    lane = lax.broadcasted_iota(jnp.int32, (1, width), 1)
    return (lane >= head * key_width) & (lane < (head + 1) * key_width)


def advanced(state, inverse_keys, weighted, sums, total_fading, key_width):
    width = state.shape[1]
    end, middle = sums[CHUNK - 1 :, :], sums[MIDDLE : MIDDLE + 1, :]
    head_count = width // key_width
    if key_width % 128 == 0:
        added = jnp.concatenate(
            [
                dot(
                    weighted[:, h * DV : (h + 1) * DV],
                    inverse_keys[:, h * key_width : (h + 1) * key_width],
                    ((0,), (0,)),
                )
                for h in range(head_count)
            ],
            axis=1,
        )
    else:
        added = jnp.zeros((DV, width), jnp.float32)
        for h in range(head_count):
            product = dot(weighted[:, h * DV : (h + 1) * DV], inverse_keys, ((0,), (0,)))
            added = jnp.where(lanes_of(h, width, key_width), product, added)
    return jnp.exp(end + total_fading) * state + jnp.exp(end - middle) * added


def remote(source, target, send, receive, device):
    return pltpu.make_async_remote_copy(
        src_ref=source,
        dst_ref=target,
        send_sem=send,
        recv_sem=receive,
        device_id=device,
        device_id_type=MESH,
    )


def rows_at(index, count):
    return pl.ds(pl.multiple_of(index * count, count), count)


class Line:
    def __init__(self, pairs, place, tp_place, whole, shards, sems, mate_sems):
        self.pairs, self.place, self.tp_place = pairs, place, tp_place
        self.pair, self.side = place // 2, place % 2
        self.gate, self.up, self.down = whole
        self.shards = shards
        self.sems, self.mate_sems = sems, mate_sems
        self.inner, self.half = shards[0].shape[0], shards[2].shape[0] // 2
        self.waited = set()
        self.issued = [0, 0]
        self.split = self.down.shape[2] % 256 == 0
        self.events = [
            (matrix, hop, piece)
            for matrix in (0, 1)
            for hop in range(1, pairs)
            for piece in self.pieces(matrix, hop)
        ]

    def pieces(self, matrix, hop):
        if not matrix:
            return range(4)
        return (0, 2, 3) if hop == self.pairs - 1 and self.split else (0, 1)

    def shard(self, kind, side):
        half = rows_at(side, self.half)
        return self.shards[kind].at[half, :] if kind == 2 else self.shards[kind].at[:, half]

    def landing(self, kind, origin):
        if kind == 2:
            return self.down.at[origin]
        return (self.up if kind else self.gate).at[rows_at(origin, self.inner), :]

    def own(self, kind):
        return self.shard(kind, self.side), self.landing(kind, self.place)

    def mate_copy(self, kind):
        return remote(
            self.shard(kind, 1 - self.side),
            self.landing(kind, self.place),
            self.mate_sems[0].at[kind],
            self.mate_sems[1].at[kind],
            (self.place + 1 - 2 * self.side, self.tp_place),
        )

    def arrive_mate(self, kind):
        if ("mate", kind) not in self.waited:
            self.waited.add(("mate", kind))
            self.mate_copy(kind).wait_recv()

    def reaches(self, way, distance):
        return self.pair + distance < self.pairs if way else self.pair >= distance

    def copy(self, way, matrix, hop, piece, distance):
        pair = (self.pair + (distance if way else -distance) + self.pairs) % self.pairs
        if matrix and piece >= 2:
            half = self.down.shape[2] // 2
            ref = self.down.at[2 * pair + 1, :, pl.ds((piece - 2) * half, half)]
        elif matrix:
            ref = self.landing(2, 2 * pair + piece)
        else:
            ref = self.landing(piece % 2, 2 * pair + (self.side if piece < 2 else 1 - self.side))
        send, receive = self.sems[matrix]
        at = (way, hop - 1, piece)
        beyond = (self.place + (-2 if way else 2) + 2 * self.pairs) % (2 * self.pairs)
        return remote(ref, ref, send.at[at], receive.at[at], (beyond, self.tp_place))

    def arrive(self, way, matrix, hop, piece):
        if (way, matrix, hop, piece) not in self.waited:
            self.waited.add((way, matrix, hop, piece))

            @pl.when(self.reaches(way, hop))
            def _():
                self.copy(way, matrix, hop, piece, hop).wait_recv()

    def passes(self, way, hop):
        return self.reaches(way, hop - 1) & self.reaches(1 - way, 1)

    def pump(self, until, ways=(0, 1)):
        count = 6 * (self.pairs - 1)
        until = len(self.events) if until >= 18 else (until * count + 17) // 18
        for way in ways:
            for matrix, hop, piece in self.events[self.issued[way] : until]:
                if hop == 1 and (matrix or piece >= 2):
                    self.arrive_mate(2 if matrix else piece % 2)
                if hop > 1:
                    self.arrive(way, matrix, hop - 1, 1 if matrix and piece else piece)

                @pl.when(self.passes(way, hop))
                def _():
                    self.copy(way, matrix, hop, piece, hop - 1).start()

            self.issued[way] = max(until, self.issued[way])

    def arrive_gates(self, until):
        for hop in range(1, until + 1):
            for piece in range(4):
                for way in (0, 1):
                    self.arrive(way, 0, hop, piece)

    def nth(self, q):
        low, high = self.pair, self.pairs - 1 - self.pair
        both = jnp.minimum(low, high)
        near = self.pair + ((q // 2) if q % 2 == 0 else -((q + 1) // 2))
        far = jnp.where(low > high, self.pair - (q - both), self.pair + (q - both))
        return jnp.where(q <= 2 * both, near, far)

    def finish(self):
        for kind in range(3):
            self.mate_copy(kind).wait_send()
        for matrix, hop, piece in self.events:
            for way in (0, 1):

                @pl.when(self.passes(way, hop))
                def _():
                    self.copy(way, matrix, hop, piece, hop - 1).wait_send()


def layer_kernel(
    n_sp,
    n_tp,
    residual_hbm,
    qa_hbm,
    qb_hbm,
    ka_hbm,
    kb_hbm,
    sa_hbm,
    sb_hbm,
    values_hbm,
    gates_hbm,
    projection_hbm,
    gate_hbm,
    up_hbm,
    down_hbm,
    fading,
    gains,
    row_gain,
    *others,
):
    outs, scratch = (others[:1], others[1:]) if down_hbm.shape[1] % 128 == 0 else (others[:2], others[2:])
    layer_body(
        n_sp,
        n_tp,
        (
            residual_hbm,
            qa_hbm,
            qb_hbm,
            ka_hbm,
            kb_hbm,
            sa_hbm,
            sb_hbm,
            values_hbm,
            gates_hbm,
            projection_hbm,
            gate_hbm,
            up_hbm,
            down_hbm,
        ),
        fading,
        gains,
        row_gain,
        outs,
        *scratch,
    )


def layer_body(
    n_sp,
    n_tp,
    in_hbm,
    fading,
    gains,
    row_gain,
    outs,
    gate_full,
    up_full,
    down_full,
    state_a,
    state_b,
    decay,
    packs,
    pair_got,
    later_got,
    terms,
    partner_terms,
    cross_terms,
    cross_got,
    all_rows,
    hidden,
    stage,
    stage_partner,
    stage_cross,
    stage_got,
    mid,
    load_sems,
    mate_send,
    mate_receive,
    gate_send,
    gate_receive,
    down_send,
    down_receive,
    pair_sems,
    later_send,
    later_receive,
    terms_send,
    terms_receive,
    cross_send,
    cross_receive,
    rows_send,
    rows_receive,
    passed_send,
    passed_receive,
    half_send,
    half_receive,
    last_send,
    last_receive,
):
    residual_hbm, qa_hbm, qb_hbm, ka_hbm, kb_hbm, sa_hbm, sb_hbm, values_hbm, gates_hbm, projection_hbm = in_hbm[:10]
    shards = in_hbm[10:]
    place, tp_place = lax.axis_index("sp"), lax.axis_index("tp")
    chip, core = tp_place // 2, tp_place % 2
    chips = n_tp // 2
    partner = (place, 2 * chip + 1 - core)
    rows, own_rows = qa_hbm.shape[0], residual_hbm.shape[0]
    chunks, units = rows // CHUNK, own_rows // CHUNK
    width_a, width_b = ka_hbm.shape[1], kb_hbm.shape[1]
    width = width_a + width_b
    odd = place % 2
    mate = place + 1 - 2 * odd
    pairs, pair_place = n_sp // 2, place // 2
    line = Line(
        pairs,
        place,
        tp_place,
        (gate_full, up_full, down_full),
        shards,
        ((gate_send, gate_receive), (down_send, down_receive)),
        (mate_send, mate_receive),
    )

    barrier = pltpu.get_barrier_semaphore()
    for k in range(1, n_sp):
        pl.semaphore_signal(
            barrier, inc=1, device_id=((place + k) % n_sp, tp_place), device_id_type=MESH
        )
    for k in range(1, n_tp):
        pl.semaphore_signal(
            barrier, inc=1, device_id=(place, (tp_place + k) % n_tp), device_id_type=MESH
        )

    for k in range(1, chips):
        pl.semaphore_signal(
            barrier,
            inc=1,
            device_id=(mate, 2 * ((chip + k) % chips) + core),
            device_id_type=MESH,
        )

    def pair_copy():
        return remote(packs.at[0], pair_got, pair_sems.at[0], pair_sems.at[1], (mate, tp_place))

    def to_later(k, slot=1):
        return remote(
            packs.at[slot],
            later_got.at[k - 1],
            later_send.at[k - 1],
            later_receive.at[k - 1],
            ((place + 2 * k) % n_sp, tp_place),
        )

    def chip_at(k):
        return (chip + 1 + k) % chips

    def terms_copy(slot):
        return remote(
            terms.at[slot], partner_terms.at[slot], terms_send.at[slot], terms_receive.at[slot], partner
        )

    def cross_copy(j, u):
        slot = j * units + u
        return remote(
            cross_terms.at[slot],
            cross_got.at[slot],
            cross_send.at[slot],
            cross_receive.at[slot],
            (place, 2 * chip_at(j) + core),
        )

    peers = [(dy, dx) for dy in (0, 1) for dx in range(chips) if dy or dx]

    def device_at(dy, dx):
        return (mate if dy else place, 2 * ((chip + dx) % chips) + core)

    def owner_at(dy, dx, of_core):
        side = 1 - odd if dy else odd
        return side * n_tp + 2 * ((chip - dx + chips) % chips) + of_core

    def own_at(owner, u):
        return all_rows.at[rows_at(owner * units + u, CHUNK), :]

    def rows_copy(k, u, owner):
        slot = k * units + u
        ref = own_at(owner, u)
        return remote(ref, ref, rows_send.at[slot], rows_receive.at[slot], device_at(*peers[k]))

    def passed_copy(k, u, owner):
        slot = k * units + u
        ref = own_at(owner, u)
        return remote(ref, ref, passed_send.at[slot], passed_receive.at[slot], partner)

    mine = owner_at(0, 0, core)
    def attention(
        residual,
        qa,
        qb,
        ka,
        kb,
        sa,
        sb,
        values,
        gates,
        projection,
        sums_a,
        sums_b,
        before_a,
        before_b,
        starts,
        heads,
        own_sum,
    ):
        groups = (
            (qa, ka, sa, sums_a, before_a, state_a, FIRST_KEY_SIZE, 0),
            (qb, kb, sb, sums_b, before_b, state_b, SECOND_KEY_SIZE, width_a),
        )

        loads = [
            line.own(0),
            line.own(1),
            (ka_hbm, ka),
            (kb_hbm, kb),
            (sa_hbm, sa),
            (sb_hbm, sb),
            (values_hbm, values),
            (qa_hbm, qa),
            (qb_hbm, qb),
            line.own(2),
            (projection_hbm, projection),
            (gates_hbm, gates),
            (residual_hbm, residual),
        ]
        loads = [pltpu.make_async_copy(a, b, load_sems.at[i]) for i, (a, b) in enumerate(loads)]
        for load in loads:
            load.start()
        state_a[...] = jnp.zeros_like(state_a)
        state_b[...] = jnp.zeros_like(state_b)
        decay[...] = jnp.zeros_like(decay)
        loads[0].wait()
        loads[1].wait()
        pl.semaphore_wait(barrier, n_sp + n_tp + chips - 3)
        line.pump(1)
        for load in loads[2:7]:
            load.wait()

        @pl.loop(0, chunks)
        def _(i):
            here = rows_at(i, CHUNK)
            column_sums, _ = fading_sums(fading[i])
            total_fading = column_sums[CHUNK - 1 :, :]
            later = jnp.exp(total_fading - column_sums)
            for group, (_, keys, switches, kept, before, state, key_width, start) in enumerate(groups):
                mine = slice(start, start + keys.shape[1])
                sums = channel_sums(switches[here, :])
                kept[here, :] = sums
                middle = sums[MIDDLE : MIDDLE + 1, :]
                inverse_keys = (keys[here, :].astype(jnp.float32) * jnp.exp(middle - sums)).astype(jnp.bfloat16)
                keys[here, :] = inverse_keys
                before[i] = (state[...] * jnp.exp(middle)).astype(jnp.bfloat16)
                starts[i, :, mine] = jnp.exp(decay[:1, mine] + middle)
                weighted = (values[group, here, :].astype(jnp.float32) * later).astype(jnp.bfloat16)
                state[...] = advanced(state[...], inverse_keys, weighted, sums, total_fading, key_width)
                decay[:, mine] += sums[CHUNK - 1 :, :] + total_fading

        def pack(slot, first, second, factor):
            packs[slot, :DV, :width_a] = first.astype(jnp.bfloat16)
            packs[slot, :DV, width_a:] = second.astype(jnp.bfloat16)
            packs[slot, DV:, :] = jnp.broadcast_to(factor, (PAD, width)).astype(jnp.bfloat16)

        whole_decay = jnp.exp(decay[:1, :])
        pack(0, state_a[...], state_b[...], whole_decay)
        pair_copy().start()
        line.mate_copy(0).start()
        line.mate_copy(1).start()
        line.pump(2, EARLY)
        pair_copy().wait_recv()
        got = pair_got[...].astype(jnp.float32)
        got_a, got_b, got_decay = got[:DV, :width_a], got[:DV, width_a:], got[DV : DV + 1, :]
        is_odd = odd == 1
        pair_a = jnp.where(
            is_odd,
            whole_decay[:, :width_a] * got_a + state_a[...],
            got_decay[:, :width_a] * state_a[...] + got_a,
        )
        pair_b = jnp.where(
            is_odd,
            whole_decay[:, width_a:] * got_b + state_b[...],
            got_decay[:, width_a:] * state_b[...] + got_b,
        )
        pack(1, pair_a, pair_b, whole_decay * got_decay)
        for k in range(1, pairs):

            @pl.when(pair_place + k < pairs - 1)
            def _():
                to_later(k).start()

        line.mate_copy(2).start()
        loads[9].wait()
        line.pump(2)
        loads[7].wait()
        loads[8].wait()

        row, column = positions()
        causal = column <= row

        @pl.loop(0, chunks)
        def _(i):
            here = rows_at(i, CHUNK)
            column_sums, row_sums = fading_sums(fading[i])
            since_start = jnp.exp(column_sums)
            between = jnp.where(causal, jnp.exp(jnp.minimum(column_sums - row_sums, 0.0)), 0.0)
            for group, (queries, keys, _, kept, before, _, key_width, _) in enumerate(groups):
                sums = kept[here, :]
                middle = sums[MIDDLE : MIDDLE + 1, :]
                spread = queries[here, :].astype(jnp.float32) * (jnp.exp(sums - middle) * key_width**-0.5)
                scaled = spread.astype(jnp.bfloat16)
                queries[here, :] = (spread * since_start).astype(jnp.bfloat16)
                inverse_keys = keys[here, :]
                local = before[i]
                for h in range(keys.shape[1] // key_width):
                    if key_width % 128 == 0:
                        mine = slice(h * key_width, (h + 1) * key_width)
                        q, k, s = scaled[:, mine], inverse_keys[:, mine], local[:, mine]
                    else:
                        q = jnp.where(lanes_of(h, keys.shape[1], key_width), scaled, jnp.zeros_like(scaled))
                        k, s = inverse_keys, local
                    scores = jnp.where(causal, dot(q, k, ((1,), (1,))) * between, 0.0).astype(jnp.bfloat16)
                    head = dot(scores, values[group, here, h * DV : (h + 1) * DV], ((1,), (0,)))
                    heads[group, here, h * DV : (h + 1) * DV] = head + since_start * dot(q, s, ((1,), (1,)))

        state_a[...] = jnp.zeros_like(state_a)
        state_b[...] = jnp.zeros_like(state_b)

        def follow(slot):
            part = slot[...].astype(jnp.float32)
            factor = part[DV : DV + 1, :]
            state_a[...] = factor[:, :width_a] * state_a[...] + part[:DV, :width_a]
            state_b[...] = factor[:, width_a:] * state_b[...] + part[:DV, width_a:]

        for k in range(pairs - 2, 0, -1):

            @pl.when((pair_place >= k) & (pair_place < pairs - 1))
            def _():
                to_later(k).wait_recv()
                follow(later_got.at[k - 1])

        if pairs > 1:

            @pl.when(pair_place == pairs - 2)
            def _():
                part = packs[1].astype(jnp.float32)
                factor = part[DV : DV + 1, :]
                pack(
                    2,
                    factor[:, :width_a] * state_a[...] + part[:DV, :width_a],
                    factor[:, width_a:] * state_b[...] + part[:DV, width_a:],
                    factor,
                )
                to_later(1, 2).start()

        line.pump(3)
        if pairs > 1:

            @pl.when(pair_place == pairs - 1)
            def _():
                to_later(1).wait_recv()
                follow(later_got.at[0])

        state_a[...] = jnp.where(is_odd, got_decay[:, :width_a] * state_a[...] + got_a, state_a[...])
        state_b[...] = jnp.where(is_odd, got_decay[:, width_a:] * state_b[...] + got_b, state_b[...])
        for load in loads[10:]:
            load.wait()

        def attend(i):
            here = rows_at(i, CHUNK)
            pieces = []
            for group, (queries, _, _, _, _, state, key_width, start) in enumerate(groups):
                key_lanes = queries.shape[1]
                earlier = (state[...] * starts[i, :, start : start + key_lanes]).astype(jnp.bfloat16)
                scaled = queries[here, :]
                for h in range(key_lanes // key_width):
                    lanes = slice(h * DV, (h + 1) * DV)
                    if key_width % 128 == 0:
                        mine = slice(h * key_width, (h + 1) * key_width)
                        q, s = scaled[:, mine], earlier[:, mine]
                    else:
                        q = jnp.where(lanes_of(h, key_lanes, key_width), scaled, jnp.zeros_like(scaled))
                        s = earlier
                    head = heads[group, here, lanes] + dot(q, s, ((1,), (1,)))
                    inverse = lax.rsqrt(jnp.mean(head * head, axis=-1, keepdims=True) + EPS)
                    gate = gates[group, here, lanes].astype(jnp.float32)
                    silu = gate / (1.0 + jnp.exp(-gate))
                    pieces.append((silu * (head * inverse * gains[group : group + 1, lanes])).astype(jnp.bfloat16))
            return dot(jnp.concatenate(pieces, axis=1), projection[...], ((1,), (0,)))

        @pl.loop(0, chips * units)
        def _(k):
            other, u = chip_at(k // units), k % units
            slot = other * units + u
            terms[slot] = attend((2 * other + 1 - core) * units + u).astype(jnp.bfloat16)
            terms_copy(slot).start()

        @pl.loop(0, (chips - 1) * units)
        def _(k):
            j, u = k // units, k % units
            other = chip_at(j)
            slot = other * units + u
            total = attend((2 * other + core) * units + u)
            terms_copy(slot).wait_recv()
            cross_terms[k] = (total + partner_terms[slot].astype(jnp.float32)).astype(jnp.bfloat16)
            cross_copy(j, u).start()

        @pl.loop(0, units)
        def _(u):
            slot = chip * units + u
            total = attend((2 * chip + core) * units + u)
            terms_copy(slot).wait_recv()
            own_sum[u] = total + partner_terms[slot].astype(jnp.float32)

        line.pump(6)

        for u in range(units):
            here = slice(u * CHUNK, (u + 1) * CHUNK)
            total = residual[here, :].astype(jnp.float32) + own_sum[u]
            for j in range(chips - 1):
                cross_copy(j, u).wait_recv()
                total = total + cross_got[j * units + u].astype(jnp.float32)
            rounded = total.astype(jnp.bfloat16)
            mid[here, :] = rounded
            widened = rounded.astype(jnp.float32)
            inverse = lax.rsqrt(jnp.mean(widened * widened, axis=-1, keepdims=True) + EPS)
            all_rows[rows_at(mine * units + u, CHUNK), :] = (widened * inverse * row_gain[...]).astype(jnp.bfloat16)
            for k in range(len(peers)):
                rows_copy(k, u, mine).start()
            passed_copy(len(peers), u, mine).start()

    pl.run_scoped(
        attention,
        *[pltpu.VMEM(a.shape, a.dtype) for a in in_hbm[:10]],
        pltpu.VMEM((rows, width_a), jnp.float32),
        pltpu.VMEM((rows, width_b), jnp.float32),
        pltpu.VMEM((chunks, DV, width_a), jnp.bfloat16),
        pltpu.VMEM((chunks, DV, width_b), jnp.bfloat16),
        pltpu.VMEM((chunks, 1, width), jnp.float32),
        pltpu.VMEM((2, rows, values_hbm.shape[2]), jnp.float32),
        pltpu.VMEM((units, CHUNK, residual_hbm.shape[1]), jnp.float32),
    )
    line.pump(8)
    for u in range(units):
        for k, peer in enumerate(peers):
            rows_copy(k, u, owner_at(*peer, core)).wait_recv()
            passed_copy(k, u, owner_at(*peer, core)).start()
        line.pump(12 + 2 * u)
    for u in range(units):
        for k, peer in enumerate(peers + [(0, 0)]):
            passed_copy(k, u, owner_at(*peer, 1 - core)).wait_recv()
    line.pump(14)
    ff = hidden.shape[1]
    tile = 256 if ff % 256 == 0 else 128
    tiles = ff // tile
    bands = 2 * chips
    band = 2 * own_rows
    last_pair = line.nth(pairs - 1)
    depth = 2 * shards[0].shape[0]
    late = rows_at(last_pair, depth)
    early = pl.ds(pl.multiple_of(jnp.where(last_pair == 0, depth, 0), depth), (pairs - 1) * depth)

    def first_half(gate_early, up_early):
        def products(n, part):
            lanes, here = rows_at(n // bands, tile), rows_at(n % bands, band)
            gate_sum = dot(all_rows[here, part], gate_full[part, lanes], ((1,), (0,)))
            return lanes, here, gate_sum, dot(all_rows[here, part], up_full[part, lanes], ((1,), (0,)))

        line.arrive_gates(pairs - 2)

        @pl.loop(0, tiles * bands)
        def _(n):
            lanes, here, gate_sum, up_sum = products(n, early)
            gate_early[here, lanes] = gate_sum
            up_early[here, lanes] = up_sum

        line.arrive_gates(pairs - 1)

        @pl.loop(0, tiles * bands)
        def _(n):
            lanes, here, gate_sum, up_sum = products(n, late)
            gate_sum, up_sum = gate_sum + gate_early[here, lanes], up_sum + up_early[here, lanes]
            hidden[here, lanes] = (gate_sum / (1.0 + jnp.exp(-gate_sum)) * up_sum).astype(jnp.bfloat16)

    pl.run_scoped(first_half, *[pltpu.VMEM(hidden.shape, jnp.float32)] * 2)

    columns = shards[2].shape[1]
    direct = columns % 128 == 0
    count = len(peers)

    order = peers[::-1] + [(0, 0)]
    order_bands = [(1 - odd if dy else odd) * chips + (chip + dx) % chips for dy, dx in order]

    blocks = [(b, 0, columns) for b in range(n_sp)]
    if line.split:
        blocks[-1:] = [(n_sp - 1, 0, columns // 2), (n_sp - 1, columns // 2, columns // 2)]
    origins = [2 * line.nth(b // 2) + b % 2 for b in range(n_sp)]

    def lanes_in(b):
        return pl.ds(0, blocks[b][2])

    def half_copy(b, k):
        at = order_bands[k]
        return remote(
            stage.at[b % DEPTH, at, 1 - core, :, lanes_in(b)],
            stage_partner.at[b, at, :, lanes_in(b)],
            half_send.at[b * (count + 1) + k],
            half_receive.at[b * (count + 1) + k],
            partner,
        )

    def last_copy(b, k):
        slot = b * count + k
        return remote(
            stage_cross.at[b % DEPTH * count + k, :, lanes_in(b)],
            stage_got.at[slot, :, lanes_in(b)],
            last_send.at[slot],
            last_receive.at[slot],
            device_at(*order[k]),
        )

    def multiply(b):
        which, start, size = blocks[b]
        for k in range(count + 1):
            if b >= DEPTH:
                half_copy(b - DEPTH, k).wait_send()
            here = rows_at(order_bands[k], band)
            part = down_full[origins[which], :, start : start + size]
            product = dot(hidden[here, :], part, ((1,), (0,))).astype(jnp.bfloat16)
            stage[b % DEPTH, order_bands[k], :, :, :size] = product.reshape(2, own_rows, size)
            half_copy(b, k).start()

    def chip_sum(b, at):
        size = blocks[b][2]
        mine_here = stage[b % DEPTH, at, core, :, :size].astype(jnp.float32)
        return mine_here + stage_partner[b, at, :, :size].astype(jnp.float32)

    def combine(b):
        for k in range(count):
            half_copy(b, k).wait_recv()
            if b >= DEPTH:
                last_copy(b - DEPTH, k).wait_send()
            both = chip_sum(b, order_bands[k]).astype(jnp.bfloat16)
            stage_cross[b % DEPTH * count + k, :, : blocks[b][2]] = both
            last_copy(b, k).start()

    def close(b):
        which, start, size = blocks[b]
        half_copy(b, count).wait_recv()
        total = chip_sum(b, odd * chips + chip)
        for k in range(count):
            last_copy(b, k).wait_recv()
            total = total + stage_got[b * count + k, :, :size].astype(jnp.float32)
        if direct:
            lanes = pl.ds(pl.multiple_of(origins[which] * columns + start, 128), size)
            outs[0][:, lanes] = (mid[:, lanes].astype(jnp.float32) + total).astype(jnp.bfloat16)
        else:
            outs[1][origins[which]] = total

    for b, (which, start, _) in enumerate(blocks):
        hop = which // 2
        if hop:
            piece = which % 2
            if piece and 2 in line.pieces(1, hop):
                piece = 3 if start else 2
            line.arrive(0, 1, hop, piece)
            line.arrive(1, 1, hop, piece)
        multiply(b)
        if b >= 1:
            combine(b - 1)
        line.pump({0: 15, 1: 16, 3: 17, 4: 18}.get(b * 8 // n_sp, 0))
        if b >= 3:
            close(b - 3)
    line.pump(18)
    combine(len(blocks) - 1)
    for b in range(len(blocks) - 3, len(blocks)):
        close(b)
    if not direct:
        outs[0][...] = mid[...]

    line.finish()
    pair_copy().wait_send()
    for k in range(1, pairs):

        @pl.when(pair_place + k < pairs - 1)
        def _():
            to_later(k).wait_send()

    if pairs > 1:

        @pl.when(pair_place == pairs - 2)
        def _():
            to_later(1, 2).wait_send()

    for slot in range(chips * units):
        terms_copy(slot).wait_send()
    for u in range(units):
        for j in range(chips - 1):
            cross_copy(j, u).wait_send()
        for k in range(count):
            rows_copy(k, u, mine).wait_send()
        for k in range(count + 1):
            passed_copy(k, u, mine).wait_send()
    for b in range(len(blocks) - DEPTH, len(blocks)):
        for k in range(count + 1):
            half_copy(b, k).wait_send()
        for k in range(count):
            last_copy(b, k).wait_send()


def per_device(
    residual,
    first_group_queries,
    first_group_keys,
    second_group_queries,
    second_group_keys,
    primary_retain_switch_inputs,
    secondary_retain_switch_inputs,
    timestep_fading_exponent,
    values,
    output_gate_logits,
    head_norm_gains,
    output_projection,
    feedforward_norm_gain,
    gate_projection,
    up_projection,
    down_projection,
):
    n_sp, n_tp = lax.axis_size("sp"), lax.axis_size("tp")
    rows, own_rows = first_group_queries.shape[0], residual.shape[0]
    features = residual.shape[1]
    chunks, units, chips = rows // CHUNK, own_rows // CHUNK, n_tp // 2
    width_a, width_b = first_group_keys.shape[1], second_group_keys.shape[1]
    width = width_a + width_b
    inner, ff = gate_projection.shape
    columns = down_projection.shape[1]
    pairs, crossings, peers = n_sp // 2, max(chips - 1, 1), 2 * chips - 1
    direct = columns % 128 == 0
    blocks = n_sp + 1 if columns % 256 == 0 else n_sp
    projection = output_projection.reshape(-1, features)
    in_hbm = [
        residual,
        first_group_queries,
        second_group_queries,
        first_group_keys,
        second_group_keys,
        primary_retain_switch_inputs,
        secondary_retain_switch_inputs,
        values,
        output_gate_logits,
        projection,
        gate_projection,
        up_projection,
        down_projection,
    ]
    in_vmem = [
        timestep_fading_exponent.reshape(chunks, 1, CHUNK),
        head_norm_gains,
        feedforward_norm_gain.reshape(1, features),
    ]

    def bf16(*shape):
        return pltpu.VMEM(shape, jnp.bfloat16)

    def f32(*shape):
        return pltpu.VMEM(shape, jnp.float32)

    def sems(*shape):
        return pltpu.SemaphoreType.DMA(shape)

    scratch = [bf16(n_sp * inner, ff // 2)] * 2 + [bf16(n_sp, ff // 2, columns)]
    scratch += [f32(DV, width_a), f32(DV, width_b), f32(8, width)]
    scratch += [bf16(3, DV + PAD, width), bf16(DV + PAD, width), bf16(max(n_sp // 2 - 1, 1), DV + PAD, width)]
    scratch += [bf16(chips * units, CHUNK, features)] * 2
    scratch += [bf16(crossings * units, CHUNK, features)] * 2
    scratch += [bf16(2 * rows, features), bf16(2 * rows, ff // 2)]
    scratch += [bf16(DEPTH, 2 * chips, 2, own_rows, columns), bf16(blocks, 2 * chips, own_rows, columns)]
    scratch += [bf16(DEPTH * peers, own_rows, columns), bf16(blocks * peers, own_rows, columns)]
    scratch += [bf16(own_rows, features)]
    scratch += [sems(len(in_hbm)), sems(3), sems(3)]
    scratch += [sems(2, max(pairs - 1, 1), 4)] * 4
    scratch += [sems(2), sems(max(n_sp // 2 - 1, 1)), sems(max(n_sp // 2 - 1, 1))]
    scratch += [sems(chips * units)] * 2
    scratch += [sems(crossings * units)] * 2
    scratch += [sems(peers * units)] * 2
    scratch += [sems((peers + 1) * units)] * 2
    scratch += [sems(blocks * (peers + 1))] * 2
    scratch += [sems(blocks * peers)] * 2
    outs = [bf16(own_rows, features)] if direct else [bf16(own_rows, features), f32(n_sp, own_rows, columns)]
    outs = pl.pallas_call(
        functools.partial(layer_kernel, n_sp, n_tp),
        in_specs=[pl.BlockSpec(memory_space=pl.ANY)] * len(in_hbm)
        + [pl.BlockSpec(memory_space=pltpu.VMEM)] * len(in_vmem),
        out_specs=[pl.BlockSpec(memory_space=pltpu.VMEM)] * len(outs),
        out_shape=outs,
        scratch_shapes=scratch,
        compiler_params=pltpu.CompilerParams(
            collective_id=0, has_side_effects=True, vmem_limit_bytes=VMEM_BYTES
        ),
        name="layer",
    )(*in_hbm, *in_vmem)
    if direct:
        return outs[0]
    added = outs[1].transpose(1, 0, 2).reshape(own_rows, features)
    return (outs[0].astype(jnp.float32) + added).astype(jnp.bfloat16)


def solution(mesh):
    return jax.shard_map(
        per_device,
        mesh=mesh,
        in_specs=(
            P(("sp", "tp"), None),
            P("sp", "tp"),
            P("sp", "tp"),
            P("sp", "tp"),
            P("sp", "tp"),
            P("sp", "tp"),
            P("sp", "tp"),
            P("sp"),
            P(None, "sp", "tp"),
            P(None, "sp", "tp"),
            P(None, "tp"),
            P(None, "tp", None),
            P(),
            P("sp", "tp"),
            P("sp", "tp"),
            P("tp", "sp"),
        ),
        out_specs=P(("sp", "tp"), None),
        check_vma=False,
    )
```

time: 189 us -> 177 us (0.937)
  Pallas kernels: 186 us -> 175 us
    pallas_call x1, Pallas kernels: 186 us -> 175 us  [per_device(): pl.pallas_call(functools.partial(layer_kernel, n_sp, n_tp), in_specs=[pl....]
where the time goes in v2:
time: 177 us; the launch traced here: 176 us
  Pallas kernels  175 us (99%)
    pallas_call x1, Pallas kernels, per_device(): pl.pallas_call(functools.partial(layer_kernel, n_sp, n_tp), in_specs=[pl....  175 us

profile of v2, /device:TPU:0, one launch (start us, length us, event | category | flops | bytes accessed | tf_op | source)
XLA Modules:
  0.0 176.4 jit_solution(2648260526313095423)
XLA Ops:
  0.0 175.4 %layer.1 = bf16[256,2048]{1,0:T(8,128)(2,1)S(1)} custom-call(bf16[256,2048]{1,0:T(8,128)(2,1)} %residual_hbm.1, bf16[1024,256]{1,0:T(8,128)(2,1)} %qa_hbm.1, bf16[1024,128]{1,0:T(8,128)(2,1)} %qb_hbm.1, bf16[1024,256]{1,0:T(8,128)(2,1)} %ka_hbm.1, bf16[1024,128]{1,0:T(8,128)(2,1)} %kb_hbm.1, bf16[1024,256]{1,0:T(8,128)(2,1)} %sa_hbm.1, ...), custom_call_target="tpu_custom_call" | custom-call | tf_op jit(solution)/shard_map/layer/pallas_call | solution.py:907
  175.5 1.0 copy.18

commit v3 on v2

--- a/solution.py
+++ b/solution.py
@@ -19,7 +19,6 @@
 SOFTNESS_SCALE = 16.0
 VMEM_BYTES = 62_000_000
 DEPTH = 4
-EARLY = (1,)
 
 def dot(a, b, dims):
     return lax.dot_general(a, b, (dims, ((), ())), preferred_element_type=jnp.float32)
@@ -170,7 +169,7 @@
     def passes(self, way, hop):
         return self.reaches(way, hop - 1) & self.reaches(1 - way, 1)
 
-    def pump(self, until, ways=(0, 1)):
+    def pump(self, until, ways=(0, 1), also=True):
         count = 6 * (self.pairs - 1)
         until = len(self.events) if until >= 18 else (until * count + 17) // 18
         for way in ways:
@@ -180,7 +179,7 @@
                 if hop > 1:
                     self.arrive(way, matrix, hop - 1, 1 if matrix and piece else piece)
 
-                @pl.when(self.passes(way, hop))
+                @pl.when(self.passes(way, hop) & also)
                 def _():
                     self.copy(way, matrix, hop, piece, hop - 1).start()
 
@@ -484,7 +483,9 @@
         pair_copy().start()
         line.mate_copy(0).start()
         line.mate_copy(1).start()
-        line.pump(2, EARLY)
+        line.pump(2, (1,))
+        calm = pair_place >= pairs - 2
+        line.pump(2, (0,), calm)
         pair_copy().wait_recv()
         got = pair_got[...].astype(jnp.float32)
         got_a, got_b, got_decay = got[:DV, :width_a], got[:DV, width_a:], got[DV : DV + 1, :]
@@ -506,9 +507,10 @@
             def _():
                 to_later(k).start()
 
+        line.issued[0] = 1
+        line.pump(2, (0,), ~calm)
         line.mate_copy(2).start()
         loads[9].wait()
-        line.pump(2)
         loads[7].wait()
         loads[8].wait()
 
@@ -657,7 +659,7 @@
         pltpu.VMEM((2, rows, values_hbm.shape[2]), jnp.float32),
         pltpu.VMEM((units, CHUNK, residual_hbm.shape[1]), jnp.float32),
     )
-    line.pump(8)
+    line.pump(10)
     for u in range(units):
         for k, peer in enumerate(peers):
             rows_copy(k, u, owner_at(*peer, core)).wait_recv()
@@ -746,20 +748,22 @@
             product = dot(hidden[here, :], part, ((1,), (0,))).astype(jnp.bfloat16)
             stage[b % DEPTH, order_bands[k], :, :, :size] = product.reshape(2, own_rows, size)
             half_copy(b, k).start()
+            if k >= 2:
+                combine(b, k - 2)
+        combine(b, count - 1)
 
     def chip_sum(b, at):
         size = blocks[b][2]
         mine_here = stage[b % DEPTH, at, core, :, :size].astype(jnp.float32)
         return mine_here + stage_partner[b, at, :, :size].astype(jnp.float32)
 
-    def combine(b):
-        for k in range(count):
-            half_copy(b, k).wait_recv()
-            if b >= DEPTH:
-                last_copy(b - DEPTH, k).wait_send()
-            both = chip_sum(b, order_bands[k]).astype(jnp.bfloat16)
-            stage_cross[b % DEPTH * count + k, :, : blocks[b][2]] = both
-            last_copy(b, k).start()
+    def combine(b, k):
+        half_copy(b, k).wait_recv()
+        if b >= DEPTH:
+            last_copy(b - DEPTH, k).wait_send()
+        both = chip_sum(b, order_bands[k]).astype(jnp.bfloat16)
+        stage_cross[b % DEPTH * count + k, :, : blocks[b][2]] = both
+        last_copy(b, k).start()
 
     def close(b):
         which, start, size = blocks[b]
@@ -783,13 +787,10 @@
             line.arrive(0, 1, hop, piece)
             line.arrive(1, 1, hop, piece)
         multiply(b)
-        if b >= 1:
-            combine(b - 1)
         line.pump({0: 15, 1: 16, 3: 17, 4: 18}.get(b * 8 // n_sp, 0))
         if b >= 3:
             close(b - 3)
     line.pump(18)
-    combine(len(blocks) - 1)
     for b in range(len(blocks) - 3, len(blocks)):
         close(b)
     if not direct:

time: 177 us -> 173 us (0.977)
  Pallas kernels: 175 us -> 172 us
    pallas_call x1, Pallas kernels: 175 us -> 172 us  [per_device(): pl.pallas_call(functools.partial(layer_kernel, n_sp, n_tp), in_specs=[pl....]
where the time goes in v3:
time: 173 us
  Pallas kernels  172 us (99%)
    pallas_call x1, Pallas kernels, per_device(): pl.pallas_call(functools.partial(layer_kernel, n_sp, n_tp), in_specs=[pl....  172 us

profile of v3, /device:TPU:0, one launch (start us, length us, event | category | flops | bytes accessed | tf_op | source)
XLA Modules:
  0.0 173.1 jit_solution(17004658953054358367)
XLA Ops:
  0.0 172.1 %layer.1 = bf16[256,2048]{1,0:T(8,128)(2,1)S(1)} custom-call(bf16[256,2048]{1,0:T(8,128)(2,1)} %residual_hbm.1, bf16[1024,256]{1,0:T(8,128)(2,1)} %qa_hbm.1, bf16[1024,128]{1,0:T(8,128)(2,1)} %qb_hbm.1, bf16[1024,256]{1,0:T(8,128)(2,1)} %ka_hbm.1, bf16[1024,128]{1,0:T(8,128)(2,1)} %kb_hbm.1, bf16[1024,256]{1,0:T(8,128)(2,1)} %sa_hbm.1, ...), custom_call_target="tpu_custom_call" | custom-call | tf_op jit(solution)/shard_map/layer/pallas_call | solution.py:908
  172.1 1.0 copy.18

commit v4 on v3

--- a/solution.py
+++ b/solution.py
@@ -19,6 +19,7 @@
 SOFTNESS_SCALE = 16.0
 VMEM_BYTES = 62_000_000
 DEPTH = 4
+QUEUE = 8
 
 def dot(a, b, dims):
     return lax.dot_general(a, b, (dims, ((), ())), preferred_element_type=jnp.float32)
@@ -153,10 +154,10 @@
             ref = self.landing(2, 2 * pair + piece)
         else:
             ref = self.landing(piece % 2, 2 * pair + (self.side if piece < 2 else 1 - self.side))
-        send, receive = self.sems[matrix]
-        at = (way, hop - 1, piece)
+        number = self.events.index((matrix, hop, piece))
+        send, receive = self.sems[0].at[way, number % QUEUE], self.sems[1].at[way, number]
         beyond = (self.place + (-2 if way else 2) + 2 * self.pairs) % (2 * self.pairs)
-        return remote(ref, ref, send.at[at], receive.at[at], (beyond, self.tp_place))
+        return remote(ref, ref, send, receive, (beyond, self.tp_place))
 
     def arrive(self, way, matrix, hop, piece):
         if (way, matrix, hop, piece) not in self.waited:
@@ -173,11 +174,14 @@
         count = 6 * (self.pairs - 1)
         until = len(self.events) if until >= 18 else (until * count + 17) // 18
         for way in ways:
-            for matrix, hop, piece in self.events[self.issued[way] : until]:
+            for number in range(self.issued[way], until):
+                matrix, hop, piece = self.events[number]
                 if hop == 1 and (matrix or piece >= 2):
                     self.arrive_mate(2 if matrix else piece % 2)
                 if hop > 1:
                     self.arrive(way, matrix, hop - 1, 1 if matrix and piece else piece)
+
+                self.left(way, number - QUEUE)
 
                 @pl.when(self.passes(way, hop) & also)
                 def _():
@@ -201,69 +205,28 @@
     def finish(self):
         for kind in range(3):
             self.mate_copy(kind).wait_send()
-        for matrix, hop, piece in self.events:
+        for number in range(len(self.events)):
             for way in (0, 1):
-
-                @pl.when(self.passes(way, hop))
-                def _():
-                    self.copy(way, matrix, hop, piece, hop - 1).wait_send()
-
-
-def layer_kernel(
-    n_sp,
-    n_tp,
-    residual_hbm,
-    qa_hbm,
-    qb_hbm,
-    ka_hbm,
-    kb_hbm,
-    sa_hbm,
-    sb_hbm,
-    values_hbm,
-    gates_hbm,
-    projection_hbm,
-    gate_hbm,
-    up_hbm,
-    down_hbm,
-    fading,
-    gains,
-    row_gain,
-    *others,
-):
-    outs, scratch = (others[:1], others[1:]) if down_hbm.shape[1] % 128 == 0 else (others[:2], others[2:])
-    layer_body(
-        n_sp,
-        n_tp,
-        (
-            residual_hbm,
-            qa_hbm,
-            qb_hbm,
-            ka_hbm,
-            kb_hbm,
-            sa_hbm,
-            sb_hbm,
-            values_hbm,
-            gates_hbm,
-            projection_hbm,
-            gate_hbm,
-            up_hbm,
-            down_hbm,
-        ),
-        fading,
-        gains,
-        row_gain,
-        outs,
-        *scratch,
-    )
+                self.left(way, number)
+
+    def left(self, way, number):
+        if number >= 0 and ("left", way, number) not in self.waited:
+            self.waited.add(("left", way, number))
+            matrix, hop, piece = self.events[number]
+
+            @pl.when(self.passes(way, hop))
+            def _():
+                self.copy(way, matrix, hop, piece, hop - 1).wait_send()
+
+
+def layer_kernel(n_sp, n_tp, in_count, out_count, *refs):
+    layer_body(n_sp, n_tp, refs[:in_count], refs[in_count : in_count + out_count], *refs[in_count + out_count :])
 
 
 def layer_body(
     n_sp,
     n_tp,
     in_hbm,
-    fading,
-    gains,
-    row_gain,
     outs,
     gate_full,
     up_full,
@@ -288,10 +251,8 @@
     load_sems,
     mate_send,
     mate_receive,
-    gate_send,
-    gate_receive,
-    down_send,
-    down_receive,
+    line_send,
+    line_receive,
     pair_sems,
     later_send,
     later_receive,
@@ -309,7 +270,8 @@
     last_receive,
 ):
     residual_hbm, qa_hbm, qb_hbm, ka_hbm, kb_hbm, sa_hbm, sb_hbm, values_hbm, gates_hbm, projection_hbm = in_hbm[:10]
-    shards = in_hbm[10:]
+    shards = in_hbm[10:13]
+    fading_hbm, gains_hbm, row_gain_hbm = in_hbm[13:]
     place, tp_place = lax.axis_index("sp"), lax.axis_index("tp")
     chip, core = tp_place // 2, tp_place % 2
     chips = n_tp // 2
@@ -327,7 +289,7 @@
         tp_place,
         (gate_full, up_full, down_full),
         shards,
-        ((gate_send, gate_receive), (down_send, down_receive)),
+        (line_send, line_receive),
         (mate_send, mate_receive),
     )
 
@@ -420,6 +382,9 @@
         starts,
         heads,
         own_sum,
+        fading,
+        gains,
+        row_gain,
     ):
         groups = (
             (qa, ka, sa, sums_a, before_a, state_a, FIRST_KEY_SIZE, 0),
@@ -429,6 +394,7 @@
         loads = [
             line.own(0),
             line.own(1),
+            (fading_hbm, fading),
             (ka_hbm, ka),
             (kb_hbm, kb),
             (sa_hbm, sa),
@@ -440,6 +406,8 @@
             (projection_hbm, projection),
             (gates_hbm, gates),
             (residual_hbm, residual),
+            (gains_hbm, gains),
+            (row_gain_hbm, row_gain),
         ]
         loads = [pltpu.make_async_copy(a, b, load_sems.at[i]) for i, (a, b) in enumerate(loads)]
         for load in loads:
@@ -451,7 +419,7 @@
         loads[1].wait()
         pl.semaphore_wait(barrier, n_sp + n_tp + chips - 3)
         line.pump(1)
-        for load in loads[2:7]:
+        for load in loads[2:8]:
             load.wait()
 
         @pl.loop(0, chunks)
@@ -510,9 +478,9 @@
         line.issued[0] = 1
         line.pump(2, (0,), ~calm)
         line.mate_copy(2).start()
+        loads[10].wait()
+        loads[8].wait()
         loads[9].wait()
-        loads[7].wait()
-        loads[8].wait()
 
         row, column = positions()
         causal = column <= row
@@ -582,7 +550,7 @@
 
         state_a[...] = jnp.where(is_odd, got_decay[:, :width_a] * state_a[...] + got_a, state_a[...])
         state_b[...] = jnp.where(is_odd, got_decay[:, width_a:] * state_b[...] + got_b, state_b[...])
-        for load in loads[10:]:
+        for load in loads[11:]:
             load.wait()
 
         def attend(i):
@@ -658,6 +626,7 @@
         pltpu.VMEM((chunks, 1, width), jnp.float32),
         pltpu.VMEM((2, rows, values_hbm.shape[2]), jnp.float32),
         pltpu.VMEM((units, CHUNK, residual_hbm.shape[1]), jnp.float32),
+        *[pltpu.VMEM(a.shape, a.dtype) for a in in_hbm[13:]],
     )
     line.pump(10)
     for u in range(units):
@@ -723,8 +692,8 @@
         return remote(
             stage.at[b % DEPTH, at, 1 - core, :, lanes_in(b)],
             stage_partner.at[b, at, :, lanes_in(b)],
-            half_send.at[b * (count + 1) + k],
-            half_receive.at[b * (count + 1) + k],
+            half_send.at[b % DEPTH * (count + 1) + k],
+            half_receive.at[b % (DEPTH + 1) * (count + 1) + k],
             partner,
         )
 
@@ -733,7 +702,7 @@
         return remote(
             stage_cross.at[b % DEPTH * count + k, :, lanes_in(b)],
             stage_got.at[slot, :, lanes_in(b)],
-            last_send.at[slot],
+            last_send.at[b % DEPTH * count + k],
             last_receive.at[slot],
             device_at(*order[k]),
         )
@@ -787,10 +756,15 @@
             line.arrive(0, 1, hop, piece)
             line.arrive(1, 1, hop, piece)
         multiply(b)
-        line.pump({0: 15, 1: 16, 3: 17, 4: 18}.get(b * 8 // n_sp, 0))
+        line.pump({0: 15, 1: 16, 3: 17}.get(b * 8 // n_sp, 0))
+        if b * 8 // n_sp == 4:
+            held = line.issued[0]
+            line.pump(18, also=core == 0)
         if b >= 3:
             close(b - 3)
-    line.pump(18)
+        if b == n_sp - 1:
+            line.issued = [held, held]
+            line.pump(18, also=core == 1)
     for b in range(len(blocks) - 3, len(blocks)):
         close(b)
     if not direct:
@@ -870,8 +844,6 @@
         gate_projection,
         up_projection,
         down_projection,
-    ]
-    in_vmem = [
         timestep_fading_exponent.reshape(chunks, 1, CHUNK),
         head_norm_gains,
         feedforward_norm_gain.reshape(1, features),
@@ -896,19 +868,18 @@
     scratch += [bf16(DEPTH * peers, own_rows, columns), bf16(blocks * peers, own_rows, columns)]
     scratch += [bf16(own_rows, features)]
     scratch += [sems(len(in_hbm)), sems(3), sems(3)]
-    scratch += [sems(2, max(pairs - 1, 1), 4)] * 4
+    scratch += [sems(2, QUEUE), sems(2, max(6 * pairs - 5, 1))]
     scratch += [sems(2), sems(max(n_sp // 2 - 1, 1)), sems(max(n_sp // 2 - 1, 1))]
     scratch += [sems(chips * units)] * 2
     scratch += [sems(crossings * units)] * 2
     scratch += [sems(peers * units)] * 2
     scratch += [sems((peers + 1) * units)] * 2
-    scratch += [sems(blocks * (peers + 1))] * 2
-    scratch += [sems(blocks * peers)] * 2
+    scratch += [sems(DEPTH * (peers + 1)), sems((DEPTH + 1) * (peers + 1))]
+    scratch += [sems(DEPTH * peers), sems(blocks * peers)]
     outs = [bf16(own_rows, features)] if direct else [bf16(own_rows, features), f32(n_sp, own_rows, columns)]
     outs = pl.pallas_call(
-        functools.partial(layer_kernel, n_sp, n_tp),
-        in_specs=[pl.BlockSpec(memory_space=pl.ANY)] * len(in_hbm)
-        + [pl.BlockSpec(memory_space=pltpu.VMEM)] * len(in_vmem),
+        functools.partial(layer_kernel, n_sp, n_tp, len(in_hbm), len(outs)),
+        in_specs=[pl.BlockSpec(memory_space=pl.ANY)] * len(in_hbm),
         out_specs=[pl.BlockSpec(memory_space=pltpu.VMEM)] * len(outs),
         out_shape=outs,
         scratch_shapes=scratch,
@@ -916,7 +887,7 @@
             collective_id=0, has_side_effects=True, vmem_limit_bytes=VMEM_BYTES
         ),
         name="layer",
-    )(*in_hbm, *in_vmem)
+    )(*in_hbm)
     if direct:
         return outs[0]
     added = outs[1].transpose(1, 0, 2).reshape(own_rows, features)

time: 173 us -> 170 us (0.983)
  Pallas kernels: 172 us -> 168 us
    pallas_call x1, Pallas kernels: 172 us -> 168 us  [per_device(): pl.pallas_call(functools.partial(layer_kernel, n_sp, n_tp, len(in_hbm), l...]
where the time goes in v4:
time: 170 us; the launch traced here: 169 us
  Pallas kernels  168 us (99%)
    pallas_call x1, Pallas kernels, per_device(): pl.pallas_call(functools.partial(layer_kernel, n_sp, n_tp, len(in_hbm), l...  168 us

profile of v4, /device:TPU:0, one launch (start us, length us, event | category | flops | bytes accessed | tf_op | source)
XLA Modules:
  0.0 169.3 jit_solution(6897956669949438218)
XLA Ops:
  0.0 168.3 %layer.1 = bf16[256,2048]{1,0:T(8,128)(2,1)S(1)} custom-call(bf16[256,2048]{1,0:T(8,128)(2,1)} %refs_0_.1, bf16[1024,256]{1,0:T(8,128)(2,1)} %refs_1_.1, bf16[1024,128]{1,0:T(8,128)(2,1)} %refs_2_.1, bf16[1024,256]{1,0:T(8,128)(2,1)} %refs_3_.1, bf16[1024,128]{1,0:T(8,128)(2,1)} %refs_4_.1, bf16[1024,256]{1,0:T(8,128)(2,1)} %refs_5_.1, ...), custom_call_target="tpu_custom_call" | custom-call | tf_op jit(solution)/shard_map/layer/pallas_call | solution.py:880
  168.3 1.0 copy.18

commit v5 on v4

--- a/solution.py
+++ b/solution.py
@@ -351,7 +351,7 @@
         return side * n_tp + 2 * ((chip - dx + chips) % chips) + of_core
 
     def own_at(owner, u):
-        return all_rows.at[rows_at(owner * units + u, CHUNK), :]
+        return all_rows.at[rows_at(u * 2 * n_tp + owner, CHUNK), :]
 
     def rows_copy(k, u, owner):
         slot = k * units + u
@@ -611,7 +611,7 @@
             mid[here, :] = rounded
             widened = rounded.astype(jnp.float32)
             inverse = lax.rsqrt(jnp.mean(widened * widened, axis=-1, keepdims=True) + EPS)
-            all_rows[rows_at(mine * units + u, CHUNK), :] = (widened * inverse * row_gain[...]).astype(jnp.bfloat16)
+            all_rows[rows_at(u * 2 * n_tp + mine, CHUNK), :] = (widened * inverse * row_gain[...]).astype(jnp.bfloat16)
             for k in range(len(peers)):
                 rows_copy(k, u, mine).start()
             passed_copy(len(peers), u, mine).start()
@@ -629,44 +629,45 @@
         *[pltpu.VMEM(a.shape, a.dtype) for a in in_hbm[13:]],
     )
     line.pump(10)
-    for u in range(units):
-        for k, peer in enumerate(peers):
-            rows_copy(k, u, owner_at(*peer, core)).wait_recv()
-            passed_copy(k, u, owner_at(*peer, core)).start()
-        line.pump(12 + 2 * u)
-    for u in range(units):
-        for k, peer in enumerate(peers + [(0, 0)]):
-            passed_copy(k, u, owner_at(*peer, 1 - core)).wait_recv()
-    line.pump(14)
     ff = hidden.shape[1]
     tile = 256 if ff % 256 == 0 else 128
     tiles = ff // tile
     bands = 2 * chips
-    band = 2 * own_rows
+    part_rows = 2 * n_tp * CHUNK
+    wide = min(512, part_rows)
+    wides = part_rows // wide
     last_pair = line.nth(pairs - 1)
     depth = 2 * shards[0].shape[0]
     late = rows_at(last_pair, depth)
     early = pl.ds(pl.multiple_of(jnp.where(last_pair == 0, depth, 0), depth), (pairs - 1) * depth)
 
     def first_half(gate_early, up_early):
-        def products(n, part):
-            lanes, here = rows_at(n // bands, tile), rows_at(n % bands, band)
+        def products(n, u, part):
+            lanes, here = rows_at(n // wides, tile), rows_at(u * wides + n % wides, wide)
             gate_sum = dot(all_rows[here, part], gate_full[part, lanes], ((1,), (0,)))
             return lanes, here, gate_sum, dot(all_rows[here, part], up_full[part, lanes], ((1,), (0,)))
 
-        line.arrive_gates(pairs - 2)
-
-        @pl.loop(0, tiles * bands)
+        for u in range(units):
+            for k, peer in enumerate(peers):
+                rows_copy(k, u, owner_at(*peer, core)).wait_recv()
+                passed_copy(k, u, owner_at(*peer, core)).start()
+            line.pump(12 + 2 * u)
+            for k, peer in enumerate(peers + [(0, 0)]):
+                passed_copy(k, u, owner_at(*peer, 1 - core)).wait_recv()
+            line.arrive_gates(pairs - 2)
+
+            @pl.loop(0, tiles * wides)
+            def _(n):
+                lanes, here, gate_sum, up_sum = products(n, u, early)
+                gate_early[here, lanes] = gate_sum
+                up_early[here, lanes] = up_sum
+
+        line.pump(14)
+        line.arrive_gates(pairs - 1)
+
+        @pl.loop(0, tiles * wides * units)
         def _(n):
-            lanes, here, gate_sum, up_sum = products(n, early)
-            gate_early[here, lanes] = gate_sum
-            up_early[here, lanes] = up_sum
-
-        line.arrive_gates(pairs - 1)
-
-        @pl.loop(0, tiles * bands)
-        def _(n):
-            lanes, here, gate_sum, up_sum = products(n, late)
+            lanes, here, gate_sum, up_sum = products(n % (tiles * wides), n // (tiles * wides), late)
             gate_sum, up_sum = gate_sum + gate_early[here, lanes], up_sum + up_early[here, lanes]
             hidden[here, lanes] = (gate_sum / (1.0 + jnp.exp(-gate_sum)) * up_sum).astype(jnp.bfloat16)
 
@@ -712,10 +713,12 @@
         for k in range(count + 1):
             if b >= DEPTH:
                 half_copy(b - DEPTH, k).wait_send()
-            here = rows_at(order_bands[k], band)
             part = down_full[origins[which], :, start : start + size]
-            product = dot(hidden[here, :], part, ((1,), (0,))).astype(jnp.bfloat16)
-            stage[b % DEPTH, order_bands[k], :, :, :size] = product.reshape(2, own_rows, size)
+            for u in range(units):
+                here = rows_at(u * bands + order_bands[k], 2 * CHUNK)
+                product = dot(hidden[here, :], part, ((1,), (0,))).astype(jnp.bfloat16)
+                lines = slice(u * CHUNK, (u + 1) * CHUNK)
+                stage[b % DEPTH, order_bands[k], :, lines, :size] = product.reshape(2, CHUNK, size)
             half_copy(b, k).start()
             if k >= 2:
                 combine(b, k - 2)
@@ -762,9 +765,8 @@
             line.pump(18, also=core == 0)
         if b >= 3:
             close(b - 3)
-        if b == n_sp - 1:
-            line.issued = [held, held]
-            line.pump(18, also=core == 1)
+    line.issued = [held, held]
+    line.pump(18, also=core == 1)
     for b in range(len(blocks) - 3, len(blocks)):
         close(b)
     if not direct:

time: 170 us -> 170 us (level)
  no operation moved by 1% of the time
where the time goes in v5:
time: 170 us
  Pallas kernels  169 us (99%)
    pallas_call x1, Pallas kernels, per_device(): pl.pallas_call(functools.partial(layer_kernel, n_sp, n_tp, len(in_hbm), l...  169 us

profile of v5, /device:TPU:0, one launch (start us, length us, event | category | flops | bytes accessed | tf_op | source)
XLA Modules:
  0.0 169.6 jit_solution(4699298413867503177)
XLA Ops:
  0.0 168.6 %layer.1 = bf16[256,2048]{1,0:T(8,128)(2,1)S(1)} custom-call(bf16[256,2048]{1,0:T(8,128)(2,1)} %refs_0_.1, bf16[1024,256]{1,0:T(8,128)(2,1)} %refs_1_.1, bf16[1024,128]{1,0:T(8,128)(2,1)} %refs_2_.1, bf16[1024,256]{1,0:T(8,128)(2,1)} %refs_3_.1, bf16[1024,128]{1,0:T(8,128)(2,1)} %refs_4_.1, bf16[1024,256]{1,0:T(8,128)(2,1)} %refs_5_.1, ...), custom_call_target="tpu_custom_call" | custom-call | tf_op jit(solution)/shard_map/layer/pallas_call | solution.py:882
  168.6 1.0 copy.18
